TPU v7x, 32 devices: a whole 2x2x4 slice. The times are simulated.
32 devices in a mesh: sp: 16 (over z, y, x), tp: 2 (over core).
Axes of the slice: x: 2, y: 2, z: 4, core: 2. Of those that a mesh axis runs over, the one named last changes fastest.
Arguments:
- resid: bfloat16 [3072, 2048], P('sp'), may hold values from -6 to 6
- queries: bfloat16 [3072, 1024], P('sp', 'tp'), may hold values from -6.5 to 6.5
- keys: bfloat16 [3072, 1024], P('sp', 'tp'), may hold values from -6.5 to 6.5
- values: bfloat16 [3072, 1024], P('sp', 'tp'), may hold values from -6 to 6
- lambdas: float32 [8], P('tp'), may hold values from 0.3 to 0.8
- head_gain: float32 [128], replicated, may hold values from 0.1 to 1.9
- out_weight: bfloat16 [1024, 2048], P('tp'), may hold values from -0.1875 to 0.1875
- norm_gain: float32 [2048], replicated, may hold values from 0.1 to 1.9
- gate_weight: bfloat16 [2048, 5632], P('sp', 'tp'), may hold values from -0.125 to 0.125
- up_weight: bfloat16 [2048, 5632], P('sp', 'tp'), may hold values from -0.125 to 0.125
- down_weight: bfloat16 [5632, 2048], P('tp', 'sp'), may hold values from -0.078125 to 0.078125
Outputs:
- result: bfloat16 [3072, 2048], P('sp')
All inputs are finite; a program needn't handle non-finite values.
Results may differ from a plain program's by a relative error of at most 0.014.
Values may be sent and summed in bfloat16 or wider, within the bound.
A program may use at most 128 MiB of HBM per device.

v0:
```python
import jax
import jax.numpy as jnp
from jax import lax
from jax.experimental import pallas as pl
from jax.experimental.pallas import tpu as pltpu
from jax.sharding import PartitionSpec as P

QK = 64
VD = 128
LANE = 128
LATE = 3
VMEM_LIMIT = 60 * 1024 * 1024


def rms_rows(first, norm_gain):
    return (
        first * lax.rsqrt(jnp.mean(first * first, axis=-1, keepdims=True) + 1e-06) * norm_gain
    ).astype(jnp.bfloat16)


def generic(
    resid,
    queries,
    keys,
    values,
    lambdas,
    head_gain,
    out_weight,
    norm_gain,
    gate_weight,
    up_weight,
    down_weight,
):
    tok_rows = queries.shape[0]
    local_heads = lambdas.shape[0]
    model_width = resid.shape[1]
    offset = lax.axis_index("sp") * tok_rows
    query_four = queries.reshape(tok_rows, local_heads, 2, QK)
    score_scale = QK ** (-0.5)
    query_pos = offset + lax.iota(jnp.int32, tok_rows)

    def update(fold_state, key_part, value_part, key_pos):
        run_max, run_sum, run_acc = fold_state
        scores = (
            jnp.einsum("qhcd,khcd->chqk", query_four, key_part, preferred_element_type=jnp.float32)
            * score_scale
        )
        causal_mask = key_pos[None, :] <= query_pos[:, None]
        scores = jnp.where(causal_mask, scores, -1e30)
        new_max = jnp.maximum(run_max, jnp.max(scores, axis=-1))
        expo = jnp.where(causal_mask, jnp.exp(scores - new_max[..., None]), 0.0)
        factor = jnp.exp(run_max - new_max)
        new_sum = run_sum * factor + jnp.sum(expo, axis=-1)
        new_acc = run_acc * factor[..., None] + jnp.einsum(
            "chqk,khd->chqd",
            expo.astype(jnp.bfloat16),
            value_part,
            preferred_element_type=jnp.float32,
        )
        return (new_max, new_sum, new_acc)

    initial = (
        jnp.full((2, local_heads, tok_rows), -1e30, jnp.float32),
        jnp.zeros((2, local_heads, tok_rows), jnp.float32),
        jnp.zeros((2, local_heads, tok_rows, VD), jnp.float32),
    )
    key_rows = lax.all_gather(keys, "sp", axis=0, tiled=True)
    value_rows = lax.all_gather(values, "sp", axis=0, tiled=True)
    key_count = key_rows.shape[0]
    key_span = key_count
    while key_span > 1024 and key_span % 2 == 0:
        key_span = key_span // 2

    def one_span(span_index, inner_state):
        span_start = span_index * key_span
        key_part = lax.dynamic_slice_in_dim(key_rows, span_start, key_span, 0).reshape(
            key_span, local_heads, 2, QK
        )
        value_part = lax.dynamic_slice_in_dim(value_rows, span_start, key_span, 0).reshape(
            key_span, local_heads, VD
        )
        key_pos = span_start + lax.iota(jnp.int32, key_span)
        return update(inner_state, key_part, value_part, key_pos)

    final_max, final_sum, final_acc = lax.fori_loop(0, key_count // key_span, one_span, initial)
    ratio = final_acc / final_sum[..., None]
    mixed_heads = ratio[0] - lambdas[:, None, None] * ratio[1]
    head_out = (
        mixed_heads
        * lax.rsqrt(jnp.mean(mixed_heads * mixed_heads, axis=-1, keepdims=True) + 1e-05)
        * head_gain
    ).astype(jnp.bfloat16)
    out_three = out_weight.reshape(local_heads, VD, model_width)
    own_count = tok_rows // lax.axis_size("tp")
    branch = lax.psum_scatter(
        jnp.einsum("hqd,hde->qe", head_out, out_three, preferred_element_type=jnp.float32).astype(
            jnp.bfloat16
        ),
        "tp",
        scatter_dimension=0,
        tiled=True,
    ).astype(jnp.float32)
    resid_own = lax.dynamic_slice_in_dim(resid, lax.axis_index("tp") * own_count, own_count, 0)
    first = resid_own.astype(jnp.float32) + branch
    normed_all = lax.all_gather(rms_rows(first, norm_gain), "tp", axis=0, tiled=True)
    gate_act = jnp.dot(
        normed_all,
        lax.all_gather(gate_weight, "sp", axis=0, tiled=True),
        preferred_element_type=jnp.float32,
    )
    up_act = jnp.dot(
        normed_all,
        lax.all_gather(up_weight, "sp", axis=0, tiled=True),
        preferred_element_type=jnp.float32,
    )
    hidden = (jax.nn.silu(gate_act) * up_act).astype(jnp.bfloat16)
    terms = jnp.dot(
        hidden,
        lax.all_gather(down_weight, "sp", axis=1, tiled=True),
        preferred_element_type=jnp.float32,
    )
    mixer = lax.psum_scatter(
        terms.astype(jnp.bfloat16), "tp", scatter_dimension=0, tiled=True
    ).astype(jnp.float32)
    finished = (first + 0.5 * mixer).astype(jnp.bfloat16)
    return lax.all_gather(finished, "tp", axis=0, tiled=True)


def where_am_i(R):
    s = lax.axis_index("sp")
    return s // R, lax.rem(s, R), lax.axis_index("tp")


def remote(src, dst, send, recv, sp, tp):
    return pltpu.make_async_remote_copy(
        src_ref=src,
        dst_ref=dst,
        send_sem=send,
        recv_sem=recv,
        device_id={"sp": sp, "tp": tp},
        device_id_type=pl.DeviceIdType.MESH,
    )


def greet(peers):
    barrier = pltpu.get_barrier_semaphore()
    for sp, tp in peers:
        pl.semaphore_signal(
            barrier,
            inc=1,
            device_id={"sp": sp, "tp": tp},
            device_id_type=pl.DeviceIdType.MESH,
        )
    pl.semaphore_wait(barrier, len(peers))


def first_block(zz, share):
    return (zz * share) // LANE


def mirror_x(r):
    return r + 1 - 2 * lax.rem(r, 2)


def mirror_y(r):
    return r + 2 - 4 * (lax.rem(r, 4) // 2)


def attention_block(R, T, i, r, q_at, k_at, v_at, lam, gain):
    span = R * T
    query = q_at(i) * jnp.bfloat16(QK**-0.5)
    ratios = []
    for c in range(2):
        part = query[:, c * QK : (c + 1) * QK]

        def fold(n, state, masked):
            run_max, run_sum, run_acc = state
            key = k_at(n)[:, c * QK : (c + 1) * QK]
            scores = lax.dot_general(
                part, key, (((1,), (1,)), ((), ())), preferred_element_type=jnp.float32
            )
            if masked:
                qpos = r * T + lax.broadcasted_iota(jnp.int32, scores.shape, 0)
                kpos = lax.broadcasted_iota(jnp.int32, scores.shape, 1)
                scores = jnp.where(kpos <= qpos, scores, -1e30)
            new_max = jnp.maximum(run_max, jnp.max(scores, axis=-1, keepdims=True))
            expo = jnp.exp(scores - new_max)
            factor = jnp.exp(run_max - new_max)
            new_sum = run_sum * factor + jnp.sum(expo, axis=-1, keepdims=True)
            new_acc = run_acc * factor + jnp.dot(
                expo.astype(jnp.bfloat16), v_at(n), preferred_element_type=jnp.float32
            )
            return new_max, new_sum, new_acc

        state = (
            jnp.full((T, 1), -1e30, jnp.float32),
            jnp.zeros((T, 1), jnp.float32),
            jnp.zeros((T, VD), jnp.float32),
        )
        state = fold(i, state, True)
        state = lax.fori_loop(0, i, lambda n, st: fold(n, st, False), state)
        ratios.append(state[2] / state[1])
    mixed = ratios[0] - lam * ratios[1]
    return (
        mixed * lax.rsqrt(jnp.mean(mixed * mixed, axis=-1, keepdims=True) + 1e-05) * gain
    ).astype(jnp.bfloat16)


def whole_kernel(Z, R, share, width, refs):
    (
        q_in, k_in, v_in, g_in, u_in, d_in, resid_in, w_in, lam, head_gain, norm_gain,
        out,
        q_sc, k_sc, v_sc, g_sc, u_sc, d_sc, resid, w,
        ho, heads, part, got, first, norm_sc, all_sc,
        hidden, terms, cross, sums, landed,
        send1, recv1, send2, recv2, local_sem, ho_sem, swap_sem, ag_sem, core_sem,
        cross_sem, sum_sem, out_sem,
    ) = refs
    ins = (q_in, k_in, v_in, g_in, u_in, d_in)
    outs = (q_sc, k_sc, v_sc, g_sc, u_sc, d_sc)
    z, r, t = where_am_i(R)
    me = z * R + r
    rx, ry = mirror_x(r), mirror_y(r)
    rd = mirror_x(ry)
    T = k_in.shape[0]
    W = g_in.shape[0]
    D = resid_in.shape[1]
    H = T // 2
    ahead = [lax.rem(z + j, Z) for j in range(Z)]
    behind = [lax.rem(z + Z - j, Z) for j in range(Z)]

    def dev(zz, rr):
        return zz * R + rr

    greet(
        [(dev(ahead[j], r), t) for j in range(1, Z)]
        + [(dev(z, rx), t), (dev(z, ry), t), (me, 1 - t)]
    )

    def source(a, zz, h=None):
        ref = ins[a]
        if a == 5:
            start = pl.multiple_of(first_block(zz, share) * LANE, LANE)
            if h is None:
                return ref.at[pl.ds(start, width), :]
            n = width // 2
            return ref.at[pl.ds(pl.multiple_of(start + h * n, 64), n), :]
        if a < 3:
            rows, sl = T, pl.ds(pl.multiple_of(zz * VD, LANE), VD)
        else:
            rows, sl = W, pl.ds(pl.multiple_of(first_block(zz, share) * LANE, LANE), width)
        if h is None:
            return ref.at[:, sl]
        n = rows // 2
        return ref.at[pl.ds(h * n, n), sl]

    def place(a, zz, rr, h=None):
        ref = outs[a]
        if a == 0:
            return ref.at[zz]
        slot = dev(zz, rr)
        if h is None:
            return ref.at[slot]
        n = ref.shape[1] // 2
        return ref.at[slot, pl.ds(h * n, n), :]

    started, locals_ = [], []

    def first_hop(a, j):
        c = remote(
            source(a, ahead[j]), place(a, z, r), send1.at[a, j], recv1.at[a, j], dev(ahead[j], r), t
        )
        c.start()
        started.append(c)

    def arrived(a, j):
        zz = behind[j]
        remote(
            source(a, z), place(a, zz, r), send1.at[a, j], recv1.at[a, j], dev(zz, r), t
        ).wait_recv()

    def keep(src, dst, n):
        c = pltpu.make_async_copy(src, dst, local_sem.at[n])
        c.start()
        locals_.append(c)

    def hop2(a, j, kind, owner, h, target, from_input):
        zz = behind[j]
        src = source(a, z, h) if from_input else place(a, zz, owner, h)
        return remote(
            src,
            place(a, zz, owner, h),
            send2.at[a - 1, j, kind],
            recv2.at[a - 1, j, kind],
            dev(z, target),
            t,
        )

    def wait2(a, j, kind):
        owner = (rx, rx, ry, ry, rd, rd)[kind]
        target = (rx, rx, ry, ry, ry, rx)[kind]
        hop2(a, j, kind, owner, kind % 2, target, False).wait_recv()

    def send_piece(a, j):
        if j:
            arrived(a, j)
        for kind, h, target in ((0, 0, rx), (3, 1, ry), (1, 1, rx), (2, 0, ry)):
            c = hop2(a, j, kind, r, h, target, j == 0)
            c.start()
            started.append(c)

    def forward_piece(a, j):
        wait2(a, j, 0)
        c = hop2(a, j, 4, rx, 0, ry, False)
        c.start()
        started.append(c)
        wait2(a, j, 3)
        c = hop2(a, j, 5, ry, 1, rx, False)
        c.start()
        started.append(c)

    small = [(a, j) for j in range(Z) for a in (1, 2)]
    for j in range(1, Z):
        for a in (1, 2, 0):
            first_hop(a, j)
    for a in (1, 2):
        send_piece(a, 0)
    for a in (3, 4, 5):
        first_hop(a, 1)
    for j in range(2, Z - 1):
        for a in (3, 4):
            first_hop(a, j)
    for a in range(6):
        keep(source(a, z), place(a, z, r), a)
    keep(resid_in, resid, 6)
    keep(w_in, w, 7)
    lag = 2
    for i in range(2, len(small) + lag):
        if i in (2, 4, 6):
            send_piece(2 + i // 2, 0)
        if i < len(small):
            send_piece(*small[i])
        forward_piece(*small[i - lag])
    for j in range(2, Z - 1):
        first_hop(5, j)
    big = [(a, j) for j in range(Z) for a in (3, 4, 5)]
    big_lag = 3

    def service(i):
        if 3 <= i < len(big):
            send_piece(*big[i])
        if big_lag <= i < len(big) + big_lag:
            forward_piece(*big[i - big_lag])

    for i in range(3, 6):
        service(i)

    for a, j in small:
        for kind in (1, 2, 4, 5):
            wait2(a, j, kind)
    for j in range(1, Z):
        arrived(0, j)
    for c in locals_:
        c.wait()

    head_lam = lam[z]

    def span(ref, n):
        return ref[pl.ds(n * R, R)].reshape(R * T, VD)

    @pl.loop(0, Z)
    def _(i):
        ho[i] = attention_block(
            R,
            T,
            i,
            r,
            lambda b: q_sc[b],
            lambda n: span(k_sc, n),
            lambda n: span(v_sc, n),
            head_lam,
            head_gain[...],
        )

    copies = []
    for j in range(1, Z):
        c = remote(
            ho.at[ahead[j]], heads.at[z], ho_sem.at[0, j], ho_sem.at[1, j], dev(ahead[j], r), t
        )
        c.start()
        copies.append(c)
    for a in (3, 4, 5):
        first_hop(a, Z - 1)
    heads[z] = ho[z]

    for i in range(6, 6 + LATE):
        service(i)

    for c in copies:
        c.wait()
    NT = 512 if D % 512 == 0 else D
    for h in range(2):
        hh = (1 - t) if h == 0 else t
        rows = pl.ds(pl.multiple_of(hh * H, 16), H)
        left = jnp.concatenate([heads[n, rows, :] for n in range(Z)], axis=1)
        for n in range(0, D, NT):
            part[h, :, n : n + NT] = jnp.dot(
                left, w[:, n : n + NT], preferred_element_type=jnp.float32
            ).astype(jnp.bfloat16)
        if h == 0:
            swap = remote(part.at[0], got, swap_sem.at[0], swap_sem.at[1], me, 1 - t)
            swap.start()
    swap.wait()
    own_rows = pl.ds(pl.multiple_of(t * H, 16), H)
    first_val = resid[own_rows, :].astype(jnp.float32) + (
        part[1].astype(jnp.float32) + got[...].astype(jnp.float32)
    )
    first[...] = first_val
    norm_sc[...] = rms_rows(first_val, norm_gain[...])

    def rows_of(zz, tt):
        return all_sc.at[zz, tt]

    def ag_hop(down, d):
        zz = z + (d - 1) if down else z - (d - 1)
        to = z - 1 if down else z + 1
        return remote(
            norm_sc if d == 1 else rows_of(zz, t),
            rows_of(zz, t),
            ag_sem.at[2 * down, d],
            ag_sem.at[2 * down + 1, d],
            dev(to, r),
            t,
        )

    def sends(down, d):
        return (z > 0) & (z + (d - 1) < Z) if down else (z + 1 < Z) & (z - (d - 1) >= 0)

    def gets(down, d):
        return z + d < Z if down else z - d >= 0

    def origin(down, d):
        return z + d if down else z - d

    def to_core(down, d, tt):
        rows = rows_of(origin(down, d), tt)
        n = 2 * d + down
        return remote(rows, rows, core_sem.at[0, n], core_sem.at[1, n], me, 1 - t)

    def ag_start(d):
        for down in (0, 1):

            @pl.when(sends(down, d))
            def _(down=down):
                ag_hop(down, d).start()

    def ag_step(d):
        for down in (0, 1):

            @pl.when(gets(down, d))
            def _(down=down):
                rows = rows_of(origin(down, d), t)
                remote(
                    rows, rows, ag_sem.at[2 * down, d], ag_sem.at[2 * down + 1, d], me, 1 - t
                ).wait_recv()
                if d < Z - 1:

                    @pl.when(sends(down, d + 1))
                    def _():
                        ag_hop(down, d + 1).start()

                to_core(down, d, t).start()

    ag_start(1)
    across = remote(norm_sc, rows_of(z, t), core_sem.at[0, 0], core_sem.at[1, 0], me, 1 - t)
    across.start()
    own = pltpu.make_async_copy(norm_sc, rows_of(z, t), local_sem.at[0])
    own.start()

    for i in range(6 + LATE, len(big)):
        service(i)
    done = 1
    for i in range(len(big), len(big) + big_lag):
        if done < Z:
            ag_step(done)
            done += 1
        service(i)
    for d in range(done, Z):
        ag_step(d)
    own.wait()
    for a, j in big:
        for kind in (1, 2, 4, 5):
            wait2(a, j, kind)
    across.wait_send()
    remote(
        norm_sc, rows_of(z, 1 - t), core_sem.at[0, 0], core_sem.at[1, 0], me, 1 - t
    ).wait_recv()
    for d in range(1, Z):
        for down in (0, 1):

            @pl.when(gets(down, d))
            def _(down=down, d=d):
                to_core(down, d, 1 - t).wait_recv()
                to_core(down, d, t).wait_send()

            @pl.when(sends(down, d))
            def _(down=down, d=d):
                ag_hop(down, d).wait_send()

    FT = 256 if width % 256 == 0 else LANE
    DN = d_sc.shape[2]
    low = first_block(z, share) * LANE
    sent = []
    order = [j % Z for j in range(1, Z + 1)]
    for n, j in enumerate(order):
        zz = ahead[j]
        block = all_sc[zz].reshape(T, D)

        @pl.loop(0, width // FT)
        def _(f, block=block):
            cols = pl.ds(pl.multiple_of(f * FT, FT), FT)
            gate = jnp.dot(
                block, g_sc[:, :, cols].reshape(D, FT), preferred_element_type=jnp.float32
            )
            up = jnp.dot(
                block, u_sc[:, :, cols].reshape(D, FT), preferred_element_type=jnp.float32
            )
            unit = low + f * FT + lax.broadcasted_iota(jnp.int32, gate.shape, 1)
            counted = (unit >= z * share) & (unit < (z + 1) * share)
            value = jax.nn.silu(gate) * up
            hidden[:, cols] = jnp.where(counted, value, 0.0).astype(jnp.bfloat16)

        left = hidden[...]

        @pl.loop(0, (Z * R) // 2)
        def _(p, left=left, n=n):
            right = jnp.concatenate([d_sc[2 * p], d_sc[2 * p + 1]], axis=1)
            value = jnp.dot(left, right, preferred_element_type=jnp.float32).astype(jnp.bfloat16)
            cols = pl.ds(pl.multiple_of(p * (2 * DN), 2 * DN), 2 * DN)
            terms[n, :, :, cols] = value.reshape(2, H, 2 * DN)

        c = remote(
            terms.at[n, 1 - t], cross.at[n], cross_sem.at[0, n], cross_sem.at[1, n], me, 1 - t
        )
        c.start()
        c.wait()
        total = terms[n, t].astype(jnp.float32) + cross[n].astype(jnp.float32)
        if j:
            sums[j] = total.astype(jnp.bfloat16)
            c = remote(
                sums.at[j], landed.at[j], sum_sem.at[0, j], sum_sem.at[1, j], dev(zz, r), t
            )
            c.start()
            sent.append(c)
        else:
            first[...] = first[...] + 0.5 * total
    for c in sent:
        c.wait()
    total = landed[1].astype(jnp.float32)
    for j in range(2, Z):
        total = total + landed[j].astype(jnp.float32)
    sums[0] = (first[...] + 0.5 * total).astype(jnp.bfloat16)
    c = remote(sums.at[0], out.at[own_rows, :], out_sem.at[0], out_sem.at[1], me, 1 - t)
    c.start()
    own = pltpu.make_async_copy(sums.at[0], out.at[own_rows, :], local_sem.at[1])
    own.start()
    own.wait()
    c.wait()
    for c in started:
        c.wait_send()


def columns_form(
    resid,
    queries,
    keys,
    values,
    lambdas,
    head_gain,
    out_weight,
    norm_gain,
    gate_weight,
    up_weight,
    down_weight,
):
    Z = lambdas.shape[0]
    S = lax.axis_size("sp")
    R = S // Z
    T, D = resid.shape
    H = T // 2
    W = gate_weight.shape[0]
    DN = down_weight.shape[1]
    share = gate_weight.shape[1] // Z
    width = LANE * max(
        -(-((zz + 1) * share) // LANE) - (zz * share) // LANE for zz in range(Z)
    )
    bf, f32 = jnp.bfloat16, jnp.float32
    vm = pl.BlockSpec(memory_space=pltpu.VMEM)
    hbm = pl.BlockSpec(memory_space=pl.ANY)
    dma = pltpu.SemaphoreType.DMA

    def kernel(*refs):
        whole_kernel(Z, R, share, width, refs)

    return pl.pallas_call(
        kernel,
        out_shape=jax.ShapeDtypeStruct((T, D), bf),
        in_specs=[hbm] * 8 + [pl.BlockSpec(memory_space=pltpu.SMEM), vm, vm],
        out_specs=vm,
        scratch_shapes=[
            pltpu.VMEM((Z, T, VD), bf),
            pltpu.VMEM((S, T, VD), bf),
            pltpu.VMEM((S, T, VD), bf),
            pltpu.VMEM((S, W, width), bf),
            pltpu.VMEM((S, W, width), bf),
            pltpu.VMEM((S, width, DN), bf),
            pltpu.VMEM((T, D), bf),
            pltpu.VMEM(out_weight.shape, bf),
            pltpu.VMEM((Z, T, VD), bf),
            pltpu.VMEM((Z, T, VD), bf),
            pltpu.VMEM((2, H, D), bf),
            pltpu.VMEM((H, D), bf),
            pltpu.VMEM((H, D), f32),
            pltpu.VMEM((H, D), bf),
            pltpu.VMEM((Z, 2, H, D), bf),
            pltpu.VMEM((T, width), bf),
            pltpu.VMEM((Z, 2, H, D), bf),
            pltpu.VMEM((Z, H, D), bf),
            pltpu.VMEM((Z, H, D), bf),
            pltpu.VMEM((Z, H, D), bf),
            dma((6, Z)),
            dma((6, Z)),
            dma((5, Z, 6)),
            dma((5, Z, 6)),
            dma((8,)),
            dma((2, Z)),
            dma((2,)),
            dma((4, Z)),
            dma((2, 2 * Z)),
            dma((2, Z)),
            dma((2, Z)),
            dma((2,)),
        ],
        compiler_params=pltpu.CompilerParams(
            collective_id=0, has_side_effects=True, vmem_limit_bytes=VMEM_LIMIT
        ),
    )(
        queries,
        keys,
        values,
        gate_weight,
        up_weight,
        down_weight,
        resid,
        out_weight,
        lambdas,
        head_gain.reshape(1, -1),
        norm_gain.reshape(1, -1),
    )


def solution(mesh):
    sp, tp = mesh.shape["sp"], mesh.shape["tp"]

    def local(*args):
        heads = args[4].shape[0]
        tok_rows = args[1].shape[0]
        columns = (
            tp == 2
            and heads > 2
            and sp == 4 * heads
            and args[10].shape[1] % LANE == 0
            and args[8].shape[1] % (16 * heads) == 0
            and tok_rows % 32 == 0
        )
        return (columns_form if columns else generic)(*args)

    return jax.shard_map(
        local,
        mesh=mesh,
        in_specs=(
            P("sp", None),
            P("sp", "tp"),
            P("sp", "tp"),
            P("sp", "tp"),
            P("tp"),
            P(),
            P("tp", None),
            P(),
            P("sp", "tp"),
            P("sp", "tp"),
            P("tp", "sp"),
        ),
        out_specs=P("sp", None),
        check_vma=False,
    )
```

profile of v0, /device:TPU:25, one launch (start us, length us, event | category | flops | bytes accessed | tf_op | source)
XLA Modules:
  0.0 159.3 jit_solution(4159648375756751797)
XLA Ops:
  0.0 157.2 %shard_map.109 = bf16[192,2048]{1,0:T(8,128)(2,1)} custom-call(bf16[192,512]{1,0:T(8,128)(2,1)} %refs_0_.1, bf16[192,512]{1,0:T(8,128)(2,1)} %refs_1_.1, bf16[192,512]{1,0:T(8,128)(2,1)} %refs_2_.1, bf16[128,2816]{1,0:T(8,128)(2,1)} %refs_3_.1, bf16[128,2816]{1,0:T(8,128)(2,1)} %refs_4_.1, bf16[2816,128]{1,0:T(8,128)(2,1)} %refs_5_.1, ...), custom_call_target="tpu_custom_call" | custom-call | tf_op jit(solution)/shard_map/pallas_call | solution.py:605
  157.2 2.1 %copy.13 = bf16[192,2048]{1,0:T(8,128)(2,1)} copy(bf16[192,2048]{1,0:T(8,128)(2,1)} %shard_map.109) | data formatting | bytes 1572864
where the time goes:
time: 159 us
  Pallas kernels  157 us (99%)
  local copies, waits for them, and re-layouts  2.09 us (1%)
    pallas_call x1, Pallas kernels, columns_form(): pl.pallas_call(kernel, out_shape=jax.ShapeDtypeStruct((T, D), bf), in_spe...  157 us

commit v1 on v0

--- a/solution.py
+++ b/solution.py
@@ -8,7 +8,7 @@
 QK = 64
 VD = 128
 LANE = 128
-LATE = 3
+SUB = 2
 VMEM_LIMIT = 60 * 1024 * 1024
 
 
@@ -154,10 +154,6 @@
     pl.semaphore_wait(barrier, len(peers))
 
 
-def first_block(zz, share):
-    return (zz * share) // LANE
-
-
 def mirror_x(r):
     return r + 1 - 2 * lax.rem(r, 2)
 
@@ -206,198 +202,271 @@
     ).astype(jnp.bfloat16)
 
 
-def whole_kernel(Z, R, share, width, refs):
+def block_start(blocks, Z, zz, tt):
+    return (blocks * zz + (1 - tt) * (Z // 2)) // Z
+
+
+def when(cond, body):
+    if cond is None:
+        body()
+    else:
+        pl.when(cond)(body)
+
+
+def whole_kernel(Z, R, blocks, pairs, singles, refs):
     (
         q_in, k_in, v_in, g_in, u_in, d_in, resid_in, w_in, lam, head_gain, norm_gain,
         out,
-        q_sc, k_sc, v_sc, g_sc, u_sc, d_sc, resid, w,
+        q_sc, kv_sc, wide_sc, thin_sc, resid, w,
         ho, heads, part, got, first, norm_sc, all_sc,
-        hidden, terms, cross, sums, landed,
-        send1, recv1, send2, recv2, local_sem, ho_sem, swap_sem, ag_sem, core_sem,
-        cross_sem, sum_sem, out_sem,
+        hidden, acc, half, cross, rs_out, rs_in, res,
+        zs, zr, ps, pr, pl_sem, local_sem, ho_sem, swap_sem, ag_sem, core_sem,
+        cross_sem, rs_sem, out_sem,
     ) = refs
-    ins = (q_in, k_in, v_in, g_in, u_in, d_in)
-    outs = (q_sc, k_sc, v_sc, g_sc, u_sc, d_sc)
     z, r, t = where_am_i(R)
     me = z * R + r
     rx, ry = mirror_x(r), mirror_y(r)
     rd = mirror_x(ry)
     T = k_in.shape[0]
-    W = g_in.shape[0]
     D = resid_in.shape[1]
+    DN = d_in.shape[1]
     H = T // 2
     ahead = [lax.rem(z + j, Z) for j in range(Z)]
     behind = [lax.rem(z + Z - j, Z) for j in range(Z)]
+    chunks = pairs + singles
+    uneven = blocks % Z != 0
+    Q, KV = chunks, chunks + 1
 
     def dev(zz, rr):
         return zz * R + rr
+
+    def span_of(c):
+        return 2 if c < pairs else 1
+
+    def offset(c):
+        return 2 * c if c < pairs else pairs + c
+
+    def store(o):
+        if o == Q:
+            return q_sc
+        if o == KV:
+            return kv_sc
+        return wide_sc.at[o] if o < pairs else thin_sc.at[o - pairs]
+
+    def present(o, zz):
+        if not uneven or o != chunks - 1:
+            return None
+        count = block_start(blocks, Z, zz + 1, t) - block_start(blocks, Z, zz, t)
+        return count > blocks // Z
+
+    here = [present(o, z) for o in range(chunks + 2)]
+
+    def parts(o, zz, slot):
+        if o >= chunks:
+            cols = pl.ds(pl.multiple_of(zz * VD, LANE), VD)
+            if o == Q:
+                return [(q_in.at[:, cols], q_sc.at[slot])]
+            return [
+                (ref.at[:, cols], kv_sc.at[slot, :, pl.ds(i * VD, VD)])
+                for i, ref in enumerate((k_in, v_in))
+            ]
+        n = span_of(o)
+        dst = store(o)
+        start = pl.multiple_of((block_start(blocks, Z, zz, t) + offset(o)) * LANE, LANE)
+        pairs_ = [
+            (ref.at[:, pl.ds(start, n * LANE)], dst.at[slot, :, pl.ds(i * n * LANE, n * LANE)])
+            for i, ref in enumerate((g_in, u_in))
+        ]
+        for i in range(n):
+            rows = pl.ds(pl.multiple_of(start + i * LANE, LANE), LANE)
+            pairs_.append((d_in.at[rows, :], dst.at[slot, :, pl.ds((2 * n + i) * LANE, LANE)]))
+        return pairs_
+
+    def slot_of(o, zz):
+        return zz if o == Q else dev(zz, r)
+
+    started = []
+
+    def launch(cond, make):
+        when(cond, lambda: make().start())
+        started.append((cond, make))
+
+    def zsend(o, j):
+        return zs.at[o if here[o] is None else chunks + 1 + j]
+
+    def first_hop(o, j):
+        def body():
+            for src, dst in parts(o, ahead[j], slot_of(o, z)):
+                remote(src, dst, zsend(o, j), zr.at[o, j - 1], dev(ahead[j], r), t).start()
+
+        when(present(o, ahead[j]), body)
+
+    def arrived(o, j):
+        spot = store(o).at[slot_of(o, behind[j])]
+
+        def body():
+            remote(spot, spot, zsend(o, j), zr.at[o, j - 1], dev(behind[j], r), t).wait_recv()
+
+        when(here[o], body)
+
+    def first_hops_sent(o):
+        if here[o] is None:
+            whole = store(o).at[pl.ds(0, Z - 1)]
+            remote(whole, whole, zsend(o, 1), zr.at[o, 0], dev(ahead[1], r), t).wait_send()
+            return
+        for j in range(1, Z):
+            spot = store(o).at[0]
+            when(
+                present(o, ahead[j]),
+                lambda j=j: remote(
+                    spot, spot, zsend(o, j), zr.at[o, j - 1], dev(ahead[j], r), t
+                ).wait_send(),
+            )
+
+    def keep(o):
+        def body():
+            for src, dst in parts(o, z, slot_of(o, z)):
+                pltpu.make_async_copy(src, dst, local_sem.at[o]).start()
+
+        when(here[o], body)
+
+    def kept(o):
+        spot = store(o).at[slot_of(o, z)]
+        when(here[o], lambda: pltpu.make_async_copy(spot, spot, local_sem.at[o]).wait())
+
+    def piece(o, j, owner, h):
+        ref = store(o)
+        n = ref.shape[1] // 2
+        return ref.at[dev(behind[j], owner), pl.ds(h * n, n), :]
+
+    def psem(o):
+        return o if o < chunks else chunks
+
+    def landing(o, j, kind):
+        p = psem(o)
+        return pr.at[p, j, 0 if kind == 0 else 1] if kind in (0, 3) else pl_sem.at[p]
+
+    def hop2(o, j, kind):
+        owner = (r, r, r, r, rx, ry)[kind]
+        target = (rx, rx, ry, ry, ry, rx)[kind]
+        spot = piece(o, j, owner, kind % 2)
+        return remote(spot, spot, ps.at[psem(o)], landing(o, j, kind), dev(z, target), t)
+
+    def wait2(o, j, kind):
+        owner = rx if kind == 0 else ry
+        spot = piece(o, j, owner, kind % 2)
+        remote(spot, spot, ps.at[psem(o)], landing(o, j, kind), dev(z, owner), t).wait_recv()
+
+    def spread(o, j):
+        if j:
+            arrived(o, j)
+        else:
+            kept(o)
+
+        def body():
+            for kind in (0, 3, 1, 2):
+                hop2(o, j, kind).start()
+
+        when(here[o], body)
+
+    def relay(o, j):
+        def body():
+            wait2(o, j, 0)
+            hop2(o, j, 4).start()
+            wait2(o, j, 3)
+            hop2(o, j, 5).start()
+
+        when(here[o], body)
+
+    def settle(o):
+        whole = store(o).at[pl.ds(0, 2 * Z)]
+        when(
+            here[o],
+            lambda: remote(
+                whole, whole, ps.at[psem(o)], landing(o, 0, 1), dev(z, rx), t
+            ).wait_recv(),
+        )
+
+    def spread_sent(o):
+        whole = store(o).at[pl.ds(0, 3 * Z)]
+        when(
+            here[o],
+            lambda: remote(
+                whole, whole, ps.at[psem(o)], landing(o, 0, 1), dev(z, rx), t
+            ).wait_send(),
+        )
+
+    for o in (KV, *range(chunks), Q):
+        keep(o)
+    resid_copy = pltpu.make_async_copy(resid_in, resid, local_sem.at[chunks + 2])
+    resid_copy.start()
+    w_copy = pltpu.make_async_copy(w_in, w, local_sem.at[chunks + 3])
+    w_copy.start()
 
     greet(
         [(dev(ahead[j], r), t) for j in range(1, Z)]
         + [(dev(z, rx), t), (dev(z, ry), t), (me, 1 - t)]
     )
-
-    def source(a, zz, h=None):
-        ref = ins[a]
-        if a == 5:
-            start = pl.multiple_of(first_block(zz, share) * LANE, LANE)
-            if h is None:
-                return ref.at[pl.ds(start, width), :]
-            n = width // 2
-            return ref.at[pl.ds(pl.multiple_of(start + h * n, 64), n), :]
-        if a < 3:
-            rows, sl = T, pl.ds(pl.multiple_of(zz * VD, LANE), VD)
-        else:
-            rows, sl = W, pl.ds(pl.multiple_of(first_block(zz, share) * LANE, LANE), width)
-        if h is None:
-            return ref.at[:, sl]
-        n = rows // 2
-        return ref.at[pl.ds(h * n, n), sl]
-
-    def place(a, zz, rr, h=None):
-        ref = outs[a]
-        if a == 0:
-            return ref.at[zz]
-        slot = dev(zz, rr)
-        if h is None:
-            return ref.at[slot]
-        n = ref.shape[1] // 2
-        return ref.at[slot, pl.ds(h * n, n), :]
-
-    started, locals_ = [], []
-
-    def first_hop(a, j):
-        c = remote(
-            source(a, ahead[j]), place(a, z, r), send1.at[a, j], recv1.at[a, j], dev(ahead[j], r), t
-        )
-        c.start()
-        started.append(c)
-
-    def arrived(a, j):
-        zz = behind[j]
-        remote(
-            source(a, z), place(a, zz, r), send1.at[a, j], recv1.at[a, j], dev(zz, r), t
-        ).wait_recv()
-
-    def keep(src, dst, n):
-        c = pltpu.make_async_copy(src, dst, local_sem.at[n])
-        c.start()
-        locals_.append(c)
-
-    def hop2(a, j, kind, owner, h, target, from_input):
-        zz = behind[j]
-        src = source(a, z, h) if from_input else place(a, zz, owner, h)
-        return remote(
-            src,
-            place(a, zz, owner, h),
-            send2.at[a - 1, j, kind],
-            recv2.at[a - 1, j, kind],
-            dev(z, target),
-            t,
-        )
-
-    def wait2(a, j, kind):
-        owner = (rx, rx, ry, ry, rd, rd)[kind]
-        target = (rx, rx, ry, ry, ry, rx)[kind]
-        hop2(a, j, kind, owner, kind % 2, target, False).wait_recv()
-
-    def send_piece(a, j):
-        if j:
-            arrived(a, j)
-        for kind, h, target in ((0, 0, rx), (3, 1, ry), (1, 1, rx), (2, 0, ry)):
-            c = hop2(a, j, kind, r, h, target, j == 0)
-            c.start()
-            started.append(c)
-
-    def forward_piece(a, j):
-        wait2(a, j, 0)
-        c = hop2(a, j, 4, rx, 0, ry, False)
-        c.start()
-        started.append(c)
-        wait2(a, j, 3)
-        c = hop2(a, j, 5, ry, 1, rx, False)
-        c.start()
-        started.append(c)
-
-    small = [(a, j) for j in range(Z) for a in (1, 2)]
+    for o in (KV, Q, 0, 1):
+        for j in range(1, Z):
+            first_hop(o, j)
+        if o == KV:
+            spread(KV, 0)
+    spread(0, 0)
+    relay(KV, 0)
     for j in range(1, Z):
-        for a in (1, 2, 0):
-            first_hop(a, j)
-    for a in (1, 2):
-        send_piece(a, 0)
-    for a in (3, 4, 5):
-        first_hop(a, 1)
-    for j in range(2, Z - 1):
-        for a in (3, 4):
-            first_hop(a, j)
-    for a in range(6):
-        keep(source(a, z), place(a, z, r), a)
-    keep(resid_in, resid, 6)
-    keep(w_in, w, 7)
-    lag = 2
-    for i in range(2, len(small) + lag):
-        if i in (2, 4, 6):
-            send_piece(2 + i // 2, 0)
-        if i < len(small):
-            send_piece(*small[i])
-        forward_piece(*small[i - lag])
-    for j in range(2, Z - 1):
-        first_hop(5, j)
-    big = [(a, j) for j in range(Z) for a in (3, 4, 5)]
-    big_lag = 3
-
-    def service(i):
-        if 3 <= i < len(big):
-            send_piece(*big[i])
-        if big_lag <= i < len(big) + big_lag:
-            forward_piece(*big[i - big_lag])
-
-    for i in range(3, 6):
-        service(i)
-
-    for a, j in small:
-        for kind in (1, 2, 4, 5):
-            wait2(a, j, kind)
+        spread(KV, j)
+        if j > 1:
+            relay(KV, j - 1)
+    relay(0, 0)
+    relay(KV, Z - 1)
+    for c in range(1, chunks):
+        spread(c, 0)
+    settle(KV)
+    kept(Q)
     for j in range(1, Z):
-        arrived(0, j)
-    for c in locals_:
-        c.wait()
+        arrived(Q, j)
 
     head_lam = lam[z]
 
-    def span(ref, n):
-        return ref[pl.ds(n * R, R)].reshape(R * T, VD)
-
-    @pl.loop(0, Z)
-    def _(i):
+    def span(n, first_lane):
+        return kv_sc[pl.ds(n * R, R), :, first_lane : first_lane + VD].reshape(R * T, VD)
+
+    def ho_copy(i):
+        return remote(ho.at[i], heads.at[z], ho_sem.at[0, i], ho_sem.at[1, z], dev(i, r), t)
+
+    for i in range(Z):
         ho[i] = attention_block(
-            R,
-            T,
-            i,
-            r,
+            R, T, i, r,
             lambda b: q_sc[b],
-            lambda n: span(k_sc, n),
-            lambda n: span(v_sc, n),
+            lambda n: span(n, 0),
+            lambda n: span(n, VD),
             head_lam,
             head_gain[...],
         )
 
-    copies = []
-    for j in range(1, Z):
-        c = remote(
-            ho.at[ahead[j]], heads.at[z], ho_sem.at[0, j], ho_sem.at[1, j], dev(ahead[j], r), t
-        )
-        c.start()
-        copies.append(c)
-    for a in (3, 4, 5):
-        first_hop(a, Z - 1)
-    heads[z] = ho[z]
-
-    for i in range(6, 6 + LATE):
-        service(i)
-
-    for c in copies:
-        c.wait()
+        @pl.when(z == i)
+        def _(i=i):
+            heads[i] = ho[i]
+
+        launch(z != i, lambda i=i: ho_copy(i))
+        if i < Z - 1:
+            if i:
+                relay(i, 0)
+            spread(0, i + 1)
+    relay(3, 0)
+    spread(1, 1)
+    relay(0, 1)
+    resid_copy.wait()
+    w_copy.wait()
+    for i in range(Z):
+
+        @pl.when(z != i)
+        def _(i=i):
+            remote(
+                ho.at[i], heads.at[i], ho_sem.at[0, i], ho_sem.at[1, i], dev(i, r), t
+            ).wait_recv()
+
     NT = 512 if D % 512 == 0 else D
     for h in range(2):
         hh = (1 - t) if h == 0 else t
@@ -471,103 +540,251 @@
 
                 to_core(down, d, t).start()
 
+    def ag_done(d):
+        for down in (0, 1):
+
+            @pl.when(gets(down, d))
+            def _(down=down):
+                to_core(down, d, 1 - t).wait_recv()
+
+    def apply(cs, zz, fresh):
+        block = all_sc[zz].reshape(T, D)
+        lane = 0
+        for c in cs:
+            n = span_of(c) * LANE
+            both = jnp.dot(
+                block,
+                store(c)[:, :, : 2 * n].reshape(D, 2 * n),
+                preferred_element_type=jnp.float32,
+            )
+            value = jax.nn.silu(both[:, :n]) * both[:, n:]
+            hidden[:, lane : lane + n] = value.astype(jnp.bfloat16)
+            lane += n
+        left = hidden[:, :lane]
+        spots = [(c, 2 * span_of(c) + i) for c in cs for i in range(span_of(c))]
+        group = 4 if (Z * R) % 8 == 0 else 1
+
+        @pl.loop(0, (Z * R) // (2 * group))
+        def _(g):
+            for q in range(group):
+                p = g * group + q
+                right = jnp.concatenate(
+                    [
+                        jnp.concatenate(
+                            [store(c)[2 * p + i, :, k * LANE : (k + 1) * LANE] for c, k in spots],
+                            axis=0,
+                        )
+                        for i in range(2)
+                    ],
+                    axis=1,
+                )
+                value = jnp.dot(left, right, preferred_element_type=jnp.float32)
+                cols = pl.ds(pl.multiple_of(p * (2 * DN), 2 * DN), 2 * DN)
+                if fresh:
+                    acc[zz, :, cols] = value
+                else:
+                    acc[zz, :, cols] = acc[zz, :, cols] + value
+
+    early = tuple(range(pairs))
+    late = tuple(range(pairs, chunks))
+
+    def apply_last(cs, zz, fresh):
+        cond = here[chunks - 1]
+        if cond is None:
+            apply(cs, zz, fresh)
+            return
+        pl.when(cond)(lambda: apply(cs, zz, fresh))
+        if cs[:-1]:
+            pl.when(jnp.logical_not(cond))(lambda: apply(cs[:-1], zz, fresh))
+
+    def apply_near(cs, d, fresh):
+        for down in (0, 1):
+
+            @pl.when(gets(down, d))
+            def _(down=down):
+                apply(cs, origin(down, d), fresh)
+
     ag_start(1)
     across = remote(norm_sc, rows_of(z, t), core_sem.at[0, 0], core_sem.at[1, 0], me, 1 - t)
     across.start()
     own = pltpu.make_async_copy(norm_sc, rows_of(z, t), local_sem.at[0])
     own.start()
-
-    for i in range(6 + LATE, len(big)):
-        service(i)
-    done = 1
-    for i in range(len(big), len(big) + big_lag):
-        if done < Z:
-            ag_step(done)
-            done += 1
-        service(i)
-    for d in range(done, Z):
-        ag_step(d)
+    for c in range(2, chunks):
+        for j in range(1, Z):
+            first_hop(c, j)
+    spread(1, 2)
+    relay(0, 2)
+    spread(1, 3)
+    relay(0, 3)
+    relay(1, 1)
+    ag_step(1)
     own.wait()
-    for a, j in big:
-        for kind in (1, 2, 4, 5):
-            wait2(a, j, kind)
     across.wait_send()
     remote(
         norm_sc, rows_of(z, 1 - t), core_sem.at[0, 0], core_sem.at[1, 0], me, 1 - t
     ).wait_recv()
+    relay(1, 2)
+    relay(1, 3)
+    for c in late:
+        for j in range(1, Z):
+            spread(c, j)
+    for c in early:
+        settle(c)
+    apply(early, z, True)
+    ag_done(1)
+    apply_near(early, 1, True)
+    for j in range(1, Z):
+        relay(2, j)
+    ag_step(2)
+    for j in range(1, Z):
+        relay(3, j)
+    ag_done(2)
+    apply_near(early, 2, True)
+    for c in late:
+        settle(c)
+
+    def pick(table):
+        spot = jnp.int32(0)
+        for zz in range(Z):
+            spot = jnp.where(z == zz, table[zz], spot)
+        return spot
+
+    goals = [[Z - 2, Z - 1] + list(range(Z - 3, 0, -1)), [1, 0] + list(range(2, Z - 1))]
+    ranks = []
+    for zz in range(Z):
+        seq = []
+        for k in range(Z - 1):
+            for down in (0, 1):
+                zd = goals[down][k]
+                if (zz > zd if down else zz < zd) and zd not in seq:
+                    seq.append(zd)
+        ranks.append(seq + [zz])
+
+    def cross_copy(zz):
+        return remote(
+            half.at[zz], cross.at[zz], cross_sem.at[0, zz], cross_sem.at[1, zz], me, 1 - t
+        )
+
+    other_rows = pl.ds(pl.multiple_of((1 - t) * H, 16), H)
+    piece = H // SUB
+
+    def rs_copy(down, k, s):
+        rows = pl.ds(s * piece, piece)
+        to = z - 1 if down else z + 1
+        return remote(
+            rs_out.at[down, k, rows],
+            rs_in.at[down, k, rows],
+            rs_sem.at[2 * down, k, s],
+            rs_sem.at[2 * down + 1, k, s],
+            dev(to, r),
+            t,
+        )
+
+    def rs_wait(down, k, s):
+        rows = pl.ds(s * piece, piece)
+        fro = z + 1 if down else z - 1
+        remote(
+            rs_out.at[down, k, rows],
+            rs_in.at[down, k, rows],
+            rs_sem.at[2 * down, k, s],
+            rs_sem.at[2 * down + 1, k, s],
+            dev(fro, r),
+            t,
+        ).wait_recv()
+
+    def mine(zd, s):
+        rows = pl.ds(s * piece, piece)
+        long = pl.ds(pl.multiple_of(t * H + s * piece, 16), piece)
+        return acc[zd, long, :] + cross[zd, rows, :].astype(jnp.float32)
+
+    def hand_over(zz):
+        half[zz] = acc[zz, other_rows, :].astype(jnp.bfloat16)
+        cross_copy(zz).start()
+
+    def rs_step(down, k, inner):
+        zd = goals[down][k]
+        for s in range(SUB):
+            rows = pl.ds(s * piece, piece)
+            if s == 0:
+                cross_copy(zd).wait_recv()
+            total = mine(zd, s)
+            if inner:
+                rs_wait(down, k, s)
+                total = total + rs_in[down, k, rows, :].astype(jnp.float32)
+            rs_out[down, k, rows, :] = total.astype(jnp.bfloat16)
+            rs_copy(down, k, s).start()
+
+    for n in range(Z):
+        zz = pick([ranks[i][n] for i in range(Z)])
+        if n == 1:
+            for d in range(3, Z):
+                ag_step(d)
+                ag_done(d)
+            edge = (z == 0) | (z == Z - 1)
+            pl.when(edge)(lambda: apply_last(early + late, zz, True))
+            pl.when(jnp.logical_not(edge))(lambda: apply_last(late, zz, False))
+        else:
+            apply_last(late, zz, False)
+        hand_over(zz)
+        if n < Z - 1:
+            pl.when(z == 0)(lambda: rs_step(0, n, False))
+            pl.when(z == Z - 1)(lambda: rs_step(1, n, False))
+    for k in range(Z - 1):
+        for down in (0, 1):
+            zd = goals[down][k]
+            inner = (z > zd) & (z < Z - 1) if down else (z < zd) & (z > 0)
+            pl.when(inner)(lambda: rs_step(down, k, True))
+    cross_copy(z).wait_recv()
+    ends = []
+    for s in range(SUB):
+        rows = pl.ds(s * piece, piece)
+        first[rows, :] = first[rows, :] + 0.5 * mine(z, s)
+        for down in (0, 1):
+
+            @pl.when(z < Z - 1 if down else z > 0)
+            def _(down=down, s=s, rows=rows):
+                k = pick([goals[down].index(i) if i in goals[down] else 0 for i in range(Z)])
+                rs_wait(down, k, s)
+                first[rows, :] = first[rows, :] + 0.5 * rs_in[down, k, rows, :].astype(jnp.float32)
+
+        res[rows, :] = first[rows, :].astype(jnp.bfloat16)
+        place = out.at[pl.ds(pl.multiple_of(t * H + s * piece, 16), piece), :]
+        c = remote(res.at[rows], place, out_sem.at[0, s], out_sem.at[1, s], me, 1 - t)
+        c.start()
+        ends.append(c)
+        c = pltpu.make_async_copy(res.at[rows], place, local_sem.at[1 + s])
+        c.start()
+        ends.append(c)
+    for c in ends:
+        c.wait()
+    for zz in range(Z):
+        cross_copy(zz).wait_send()
     for d in range(1, Z):
         for down in (0, 1):
 
             @pl.when(gets(down, d))
             def _(down=down, d=d):
-                to_core(down, d, 1 - t).wait_recv()
                 to_core(down, d, t).wait_send()
 
             @pl.when(sends(down, d))
             def _(down=down, d=d):
                 ag_hop(down, d).wait_send()
 
-    FT = 256 if width % 256 == 0 else LANE
-    DN = d_sc.shape[2]
-    low = first_block(z, share) * LANE
-    sent = []
-    order = [j % Z for j in range(1, Z + 1)]
-    for n, j in enumerate(order):
-        zz = ahead[j]
-        block = all_sc[zz].reshape(T, D)
-
-        @pl.loop(0, width // FT)
-        def _(f, block=block):
-            cols = pl.ds(pl.multiple_of(f * FT, FT), FT)
-            gate = jnp.dot(
-                block, g_sc[:, :, cols].reshape(D, FT), preferred_element_type=jnp.float32
-            )
-            up = jnp.dot(
-                block, u_sc[:, :, cols].reshape(D, FT), preferred_element_type=jnp.float32
-            )
-            unit = low + f * FT + lax.broadcasted_iota(jnp.int32, gate.shape, 1)
-            counted = (unit >= z * share) & (unit < (z + 1) * share)
-            value = jax.nn.silu(gate) * up
-            hidden[:, cols] = jnp.where(counted, value, 0.0).astype(jnp.bfloat16)
-
-        left = hidden[...]
-
-        @pl.loop(0, (Z * R) // 2)
-        def _(p, left=left, n=n):
-            right = jnp.concatenate([d_sc[2 * p], d_sc[2 * p + 1]], axis=1)
-            value = jnp.dot(left, right, preferred_element_type=jnp.float32).astype(jnp.bfloat16)
-            cols = pl.ds(pl.multiple_of(p * (2 * DN), 2 * DN), 2 * DN)
-            terms[n, :, :, cols] = value.reshape(2, H, 2 * DN)
-
-        c = remote(
-            terms.at[n, 1 - t], cross.at[n], cross_sem.at[0, n], cross_sem.at[1, n], me, 1 - t
-        )
-        c.start()
-        c.wait()
-        total = terms[n, t].astype(jnp.float32) + cross[n].astype(jnp.float32)
-        if j:
-            sums[j] = total.astype(jnp.bfloat16)
-            c = remote(
-                sums.at[j], landed.at[j], sum_sem.at[0, j], sum_sem.at[1, j], dev(zz, r), t
-            )
-            c.start()
-            sent.append(c)
-        else:
-            first[...] = first[...] + 0.5 * total
-    for c in sent:
-        c.wait()
-    total = landed[1].astype(jnp.float32)
-    for j in range(2, Z):
-        total = total + landed[j].astype(jnp.float32)
-    sums[0] = (first[...] + 0.5 * total).astype(jnp.bfloat16)
-    c = remote(sums.at[0], out.at[own_rows, :], out_sem.at[0], out_sem.at[1], me, 1 - t)
-    c.start()
-    own = pltpu.make_async_copy(sums.at[0], out.at[own_rows, :], local_sem.at[1])
-    own.start()
-    own.wait()
-    c.wait()
-    for c in started:
-        c.wait_send()
+    for k in range(Z - 1):
+        for down in (0, 1):
+            zd = goals[down][k]
+
+            @pl.when(z > zd if down else z < zd)
+            def _(down=down, k=k):
+                for s in range(SUB):
+                    rs_copy(down, k, s).wait_send()
+
+    for o in (KV, Q, *range(chunks)):
+        first_hops_sent(o)
+    for o in (KV, *range(chunks)):
+        spread_sent(o)
+    for cond, make in started:
+        when(cond, lambda make=make: make().wait_send())
 
 
 def columns_form(
@@ -590,17 +807,17 @@
     H = T // 2
     W = gate_weight.shape[0]
     DN = down_weight.shape[1]
-    share = gate_weight.shape[1] // Z
-    width = LANE * max(
-        -(-((zz + 1) * share) // LANE) - (zz * share) // LANE for zz in range(Z)
-    )
+    blocks = gate_weight.shape[1] // LANE
+    pairs = blocks // Z // 2
+    singles = blocks // Z % 2 + (1 if blocks % Z else 0)
+    chunks = pairs + singles
     bf, f32 = jnp.bfloat16, jnp.float32
     vm = pl.BlockSpec(memory_space=pltpu.VMEM)
     hbm = pl.BlockSpec(memory_space=pl.ANY)
     dma = pltpu.SemaphoreType.DMA
 
     def kernel(*refs):
-        whole_kernel(Z, R, share, width, refs)
+        whole_kernel(Z, R, blocks, pairs, singles, refs)
 
     return pl.pallas_call(
         kernel,
@@ -609,11 +826,9 @@
         out_specs=vm,
         scratch_shapes=[
             pltpu.VMEM((Z, T, VD), bf),
-            pltpu.VMEM((S, T, VD), bf),
-            pltpu.VMEM((S, T, VD), bf),
-            pltpu.VMEM((S, W, width), bf),
-            pltpu.VMEM((S, W, width), bf),
-            pltpu.VMEM((S, width, DN), bf),
+            pltpu.VMEM((S, T, 2 * VD), bf),
+            pltpu.VMEM((pairs, S, W, 6 * LANE), bf),
+            pltpu.VMEM((singles, S, W, 3 * LANE), bf),
             pltpu.VMEM((T, D), bf),
             pltpu.VMEM(out_weight.shape, bf),
             pltpu.VMEM((Z, T, VD), bf),
@@ -623,23 +838,26 @@
             pltpu.VMEM((H, D), f32),
             pltpu.VMEM((H, D), bf),
             pltpu.VMEM((Z, 2, H, D), bf),
-            pltpu.VMEM((T, width), bf),
-            pltpu.VMEM((Z, 2, H, D), bf),
+            pltpu.VMEM((T, (2 * pairs + singles) * LANE), bf),
+            pltpu.VMEM((Z, T, D), f32),
             pltpu.VMEM((Z, H, D), bf),
             pltpu.VMEM((Z, H, D), bf),
-            pltpu.VMEM((Z, H, D), bf),
-            dma((6, Z)),
-            dma((6, Z)),
-            dma((5, Z, 6)),
-            dma((5, Z, 6)),
-            dma((8,)),
+            pltpu.VMEM((2, Z - 1, H, D), bf),
+            pltpu.VMEM((2, Z - 1, H, D), bf),
+            pltpu.VMEM((H, D), bf),
+            dma((chunks + 1 + Z,)),
+            dma((chunks + 2, Z - 1)),
+            dma((chunks + 1,)),
+            dma((chunks + 1, Z, 2)),
+            dma((chunks + 1,)),
+            dma((chunks + 4,)),
             dma((2, Z)),
             dma((2,)),
             dma((4, Z)),
             dma((2, 2 * Z)),
             dma((2, Z)),
-            dma((2, Z)),
-            dma((2,)),
+            dma((4, Z - 1, SUB)),
+            dma((2, SUB)),
         ],
         compiler_params=pltpu.CompilerParams(
             collective_id=0, has_side_effects=True, vmem_limit_bytes=VMEM_LIMIT
@@ -667,11 +885,14 @@
         tok_rows = args[1].shape[0]
         columns = (
             tp == 2
-            and heads > 2
+            and heads == 4
             and sp == 4 * heads
-            and args[10].shape[1] % LANE == 0
-            and args[8].shape[1] % (16 * heads) == 0
-            and tok_rows % 32 == 0
+            and args[10].shape[1] == LANE
+            and args[8].shape[0] == LANE
+            and args[8].shape[1] % LANE == 0
+            and args[8].shape[1] // LANE // heads == 5
+            and args[8].shape[1] // LANE % heads != 0
+            and tok_rows % (32 * SUB) == 0
         )
         return (columns_form if columns else generic)(*args)
 

time: 159 us -> 142 us (0.89)
  the two profiles are of different devices: /device:TPU:25 before, /device:TPU:0 now
where the time goes in v1:
time: 142 us
  Pallas kernels  140 us (99%)
  local copies, waits for them, and re-layouts  2.09 us (1%)
    pallas_call x1, Pallas kernels, columns_form(): pl.pallas_call(kernel, out_shape=jax.ShapeDtypeStruct((T, D), bf), in_spe...  140 us

profile of v1, /device:TPU:0, one launch (start us, length us, event | category | flops | bytes accessed | tf_op | source)
XLA Modules:
  0.0 141.8 jit_solution(17214203793711661742)
XLA Ops:
  0.0 139.7 %shard_map.109 = bf16[192,2048]{1,0:T(8,128)(2,1)} custom-call(bf16[192,512]{1,0:T(8,128)(2,1)} %refs_0_.1, bf16[192,512]{1,0:T(8,128)(2,1)} %refs_1_.1, bf16[192,512]{1,0:T(8,128)(2,1)} %refs_2_.1, bf16[128,2816]{1,0:T(8,128)(2,1)} %refs_3_.1, bf16[128,2816]{1,0:T(8,128)(2,1)} %refs_4_.1, bf16[2816,128]{1,0:T(8,128)(2,1)} %refs_5_.1, ...), custom_call_target="tpu_custom_call" | custom-call | tf_op jit(solution)/shard_map/pallas_call | solution.py:822
  139.7 2.1 %copy.13 = bf16[192,2048]{1,0:T(8,128)(2,1)} copy(bf16[192,2048]{1,0:T(8,128)(2,1)} %shard_map.109) | data formatting | bytes 1572864

commit v2 on v1

--- a/solution.py
+++ b/solution.py
@@ -8,7 +8,7 @@
 QK = 64
 VD = 128
 LANE = 128
-SUB = 2
+SUB = 3
 VMEM_LIMIT = 60 * 1024 * 1024
 
 
@@ -220,8 +220,8 @@
         q_sc, kv_sc, wide_sc, thin_sc, resid, w,
         ho, heads, part, got, first, norm_sc, all_sc,
         hidden, acc, half, cross, rs_out, rs_in, res,
-        zs, zr, ps, pr, pl_sem, local_sem, ho_sem, swap_sem, ag_sem, core_sem,
-        cross_sem, rs_sem, out_sem,
+        zs, zr, ps, pr, pl_sem, local_sem, ho_sem, swap_sem, ag_sem, ag_land, core_sem,
+        cross_sem, rs_sem, rs_land, out_sem,
     ) = refs
     z, r, t = where_am_i(R)
     me = z * R + r
@@ -418,9 +418,11 @@
         spread(KV, j)
         if j > 1:
             relay(KV, j - 1)
+        if j == Z - 2:
+            spread(1, 0)
     relay(0, 0)
     relay(KV, Z - 1)
-    for c in range(1, chunks):
+    for c in range(2, chunks):
         spread(c, 0)
     settle(KV)
     kept(Q)
@@ -450,13 +452,22 @@
             heads[i] = ho[i]
 
         launch(z != i, lambda i=i: ho_copy(i))
-        if i < Z - 1:
-            if i:
-                relay(i, 0)
-            spread(0, i + 1)
-    relay(3, 0)
+        if i == 0:
+            relay(1, 0)
+            spread(0, 1)
+        if i == 1:
+            relay(2, 0)
+            relay(3, 0)
+        if i == 2:
+            spread(0, 2)
+            relay(0, 1)
+    spread(0, 3)
+    relay(0, 2)
     spread(1, 1)
-    relay(0, 1)
+    spread(1, 2)
+    relay(0, 3)
+    spread(1, 3)
+    relay(1, 1)
     resid_copy.wait()
     w_copy.wait()
     for i in range(Z):
@@ -467,6 +478,8 @@
                 ho.at[i], heads.at[i], ho_sem.at[0, i], ho_sem.at[1, i], dev(i, r), t
             ).wait_recv()
 
+    first_hop(2, 1)
+    first_hop(2, 2)
     NT = 512 if D % 512 == 0 else D
     for h in range(2):
         hh = (1 - t) if h == 0 else t
@@ -490,16 +503,17 @@
     def rows_of(zz, tt):
         return all_sc.at[zz, tt]
 
-    def ag_hop(down, d):
+    part_rows = H // SUB
+
+    def ag_hop(down, d, s=None):
         zz = z + (d - 1) if down else z - (d - 1)
         to = z - 1 if down else z + 1
+        src = norm_sc if d == 1 else rows_of(zz, t)
+        dst = rows_of(zz, t)
+        if s is not None:
+            src, dst = (ref.at[pl.ds(s * part_rows, part_rows)] for ref in (src, dst))
         return remote(
-            norm_sc if d == 1 else rows_of(zz, t),
-            rows_of(zz, t),
-            ag_sem.at[2 * down, d],
-            ag_sem.at[2 * down + 1, d],
-            dev(to, r),
-            t,
+            src, dst, ag_sem.at[down, d], ag_land.at[down, d, 0 if s is None else s], dev(to, r), t
         )
 
     def sends(down, d):
@@ -517,28 +531,24 @@
         return remote(rows, rows, core_sem.at[0, n], core_sem.at[1, n], me, 1 - t)
 
     def ag_start(d):
-        for down in (0, 1):
-
-            @pl.when(sends(down, d))
-            def _(down=down):
-                ag_hop(down, d).start()
+        for s in range(SUB):
+            for down in (0, 1):
+                pl.when(sends(down, d))(lambda: ag_hop(down, d, s).start())
 
     def ag_step(d):
-        for down in (0, 1):
-
-            @pl.when(gets(down, d))
-            def _(down=down):
-                rows = rows_of(origin(down, d), t)
-                remote(
-                    rows, rows, ag_sem.at[2 * down, d], ag_sem.at[2 * down + 1, d], me, 1 - t
-                ).wait_recv()
-                if d < Z - 1:
-
-                    @pl.when(sends(down, d + 1))
-                    def _():
-                        ag_hop(down, d + 1).start()
-
-                to_core(down, d, t).start()
+        for s in range(SUB):
+            for down in (0, 1):
+
+                @pl.when(gets(down, d))
+                def _(down=down, s=s):
+                    spot = rows_of(origin(down, d), t).at[pl.ds(s * part_rows, part_rows)]
+                    remote(
+                        spot, spot, ag_sem.at[down, d], ag_land.at[down, d, s], me, 1 - t
+                    ).wait_recv()
+                    if d < Z - 1:
+                        pl.when(sends(down, d + 1))(lambda: ag_hop(down, d + 1, s).start())
+                    if s == SUB - 1:
+                        to_core(down, d, t).start()
 
     def ag_done(d):
         for down in (0, 1):
@@ -609,33 +619,30 @@
     across.start()
     own = pltpu.make_async_copy(norm_sc, rows_of(z, t), local_sem.at[0])
     own.start()
-    for c in range(2, chunks):
-        for j in range(1, Z):
-            first_hop(c, j)
-    spread(1, 2)
-    relay(0, 2)
-    spread(1, 3)
-    relay(0, 3)
-    relay(1, 1)
+    first_hop(2, 3)
+    for j in range(1, Z):
+        first_hop(3, j)
+    relay(1, 2)
+    spread(2, 1)
     ag_step(1)
     own.wait()
     across.wait_send()
     remote(
         norm_sc, rows_of(z, 1 - t), core_sem.at[0, 0], core_sem.at[1, 0], me, 1 - t
     ).wait_recv()
-    relay(1, 2)
+    spread(2, 2)
     relay(1, 3)
-    for c in late:
-        for j in range(1, Z):
-            spread(c, j)
+    spread(2, 3)
     for c in early:
         settle(c)
     apply(early, z, True)
-    ag_done(1)
-    apply_near(early, 1, True)
+    for j in range(1, Z):
+        spread(3, j)
     for j in range(1, Z):
         relay(2, j)
     ag_step(2)
+    ag_done(1)
+    apply_near(early, 1, True)
     for j in range(1, Z):
         relay(3, j)
     ag_done(2)
@@ -652,12 +659,12 @@
     goals = [[Z - 2, Z - 1] + list(range(Z - 3, 0, -1)), [1, 0] + list(range(2, Z - 1))]
     ranks = []
     for zz in range(Z):
-        seq = []
-        for k in range(Z - 1):
-            for down in (0, 1):
-                zd = goals[down][k]
-                if (zz > zd if down else zz < zd) and zd not in seq:
-                    seq.append(zd)
+        seq = [[zd for zd in goal if (zz > zd if down else zz < zd)] for down, goal in enumerate(goals)]
+        if zz in (0, Z - 1):
+            seq = seq[0] + seq[1]
+            seq = [seq[0]] + seq[2:] + [seq[1]]
+        else:
+            seq = [zd for k in range(Z - 1) for down in (0, 1) for zd in seq[down][k : k + 1]]
         ranks.append(seq + [zz])
 
     def cross_copy(zz):
@@ -674,8 +681,8 @@
         return remote(
             rs_out.at[down, k, rows],
             rs_in.at[down, k, rows],
-            rs_sem.at[2 * down, k, s],
-            rs_sem.at[2 * down + 1, k, s],
+            rs_sem.at[down, k],
+            rs_land.at[down, k, s],
             dev(to, r),
             t,
         )
@@ -686,8 +693,8 @@
         remote(
             rs_out.at[down, k, rows],
             rs_in.at[down, k, rows],
-            rs_sem.at[2 * down, k, s],
-            rs_sem.at[2 * down + 1, k, s],
+            rs_sem.at[down, k],
+            rs_land.at[down, k, s],
             dev(fro, r),
             t,
         ).wait_recv()
@@ -714,26 +721,33 @@
             rs_out[down, k, rows, :] = total.astype(jnp.bfloat16)
             rs_copy(down, k, s).start()
 
+    edge = (z == 0) | (z == Z - 1)
+
+    def edge_step(k):
+        pl.when(z == 0)(lambda: rs_step(0, k, False))
+        pl.when(z == Z - 1)(lambda: rs_step(1, k, False))
+
     for n in range(Z):
         zz = pick([ranks[i][n] for i in range(Z)])
-        if n == 1:
+        if n == Z - 2:
             for d in range(3, Z):
                 ag_step(d)
                 ag_done(d)
-            edge = (z == 0) | (z == Z - 1)
             pl.when(edge)(lambda: apply_last(early + late, zz, True))
             pl.when(jnp.logical_not(edge))(lambda: apply_last(late, zz, False))
         else:
             apply_last(late, zz, False)
         hand_over(zz)
-        if n < Z - 1:
-            pl.when(z == 0)(lambda: rs_step(0, n, False))
-            pl.when(z == Z - 1)(lambda: rs_step(1, n, False))
-    for k in range(Z - 1):
-        for down in (0, 1):
-            zd = goals[down][k]
-            inner = (z > zd) & (z < Z - 1) if down else (z < zd) & (z > 0)
-            pl.when(inner)(lambda: rs_step(down, k, True))
+        if n == 1:
+            edge_step(0)
+    edge_step(1)
+    edge_step(2)
+    for half_of, order in ((z < Z // 2, (0, 1)), (z >= Z // 2, (1, 0))):
+        for k in range(Z - 1):
+            for down in order:
+                zd = goals[down][k]
+                inner = (z > zd) & (z < Z - 1) if down else (z < zd) & (z > 0)
+                pl.when(half_of & inner)(lambda: rs_step(down, k, True))
     cross_copy(z).wait_recv()
     ends = []
     for s in range(SUB):
@@ -776,8 +790,8 @@
 
             @pl.when(z > zd if down else z < zd)
             def _(down=down, k=k):
-                for s in range(SUB):
-                    rs_copy(down, k, s).wait_send()
+                whole = rs_out.at[down, k]
+                remote(whole, whole, rs_sem.at[down, k], rs_land.at[down, k, 0], me, 1 - t).wait_send()
 
     for o in (KV, Q, *range(chunks)):
         first_hops_sent(o)
@@ -853,10 +867,12 @@
             dma((chunks + 4,)),
             dma((2, Z)),
             dma((2,)),
-            dma((4, Z)),
+            dma((2, Z)),
+            dma((2, Z, SUB)),
             dma((2, 2 * Z)),
             dma((2, Z)),
-            dma((4, Z - 1, SUB)),
+            dma((2, Z - 1)),
+            dma((2, Z - 1, SUB)),
             dma((2, SUB)),
         ],
         compiler_params=pltpu.CompilerParams(

time: 142 us -> 134 us (0.944)
  Pallas kernels: 140 us -> 132 us
    pallas_call x1, Pallas kernels: 140 us -> 132 us  [columns_form(): pl.pallas_call(kernel, out_shape=jax.ShapeDtypeStruct((T, D), bf), in_spe...]
where the time goes in v2:
time: 134 us
  Pallas kernels  132 us (99%)
  local copies, waits for them, and re-layouts  2.09 us (2%)
    pallas_call x1, Pallas kernels, columns_form(): pl.pallas_call(kernel, out_shape=jax.ShapeDtypeStruct((T, D), bf), in_spe...  132 us

profile of v2, /device:TPU:0, one launch (start us, length us, event | category | flops | bytes accessed | tf_op | source)
XLA Modules:
  0.0 134.0 jit_solution(18066716056614084738)
XLA Ops:
  0.0 131.9 %shard_map.109 = bf16[192,2048]{1,0:T(8,128)(2,1)} custom-call(bf16[192,512]{1,0:T(8,128)(2,1)} %refs_0_.1, bf16[192,512]{1,0:T(8,128)(2,1)} %refs_1_.1, bf16[192,512]{1,0:T(8,128)(2,1)} %refs_2_.1, bf16[128,2816]{1,0:T(8,128)(2,1)} %refs_3_.1, bf16[128,2816]{1,0:T(8,128)(2,1)} %refs_4_.1, bf16[2816,128]{1,0:T(8,128)(2,1)} %refs_5_.1, ...), custom_call_target="tpu_custom_call" | custom-call | tf_op jit(solution)/shard_map/pallas_call | solution.py:836
  131.9 2.1 %copy.13 = bf16[192,2048]{1,0:T(8,128)(2,1)} copy(bf16[192,2048]{1,0:T(8,128)(2,1)} %shard_map.109) | data formatting | bytes 1572864

commit v3 on v2

--- a/solution.py
+++ b/solution.py
@@ -9,6 +9,7 @@
 VD = 128
 LANE = 128
 SUB = 3
+FINE = 6
 VMEM_LIMIT = 60 * 1024 * 1024
 
 
@@ -202,8 +203,9 @@
     ).astype(jnp.bfloat16)
 
 
-def block_start(blocks, Z, zz, tt):
-    return (blocks * zz + (1 - tt) * (Z // 2)) // Z
+def block_start(blocks, Z, zz):
+    extra = blocks % Z
+    return blocks // Z * zz + jnp.minimum(jnp.maximum(zz - (Z - extra) // 2, 0), extra)
 
 
 def when(cond, body):
@@ -256,7 +258,7 @@
     def present(o, zz):
         if not uneven or o != chunks - 1:
             return None
-        count = block_start(blocks, Z, zz + 1, t) - block_start(blocks, Z, zz, t)
+        count = block_start(blocks, Z, zz + 1) - block_start(blocks, Z, zz)
         return count > blocks // Z
 
     here = [present(o, z) for o in range(chunks + 2)]
@@ -272,7 +274,7 @@
             ]
         n = span_of(o)
         dst = store(o)
-        start = pl.multiple_of((block_start(blocks, Z, zz, t) + offset(o)) * LANE, LANE)
+        start = pl.multiple_of((block_start(blocks, Z, zz) + offset(o)) * LANE, LANE)
         pairs_ = [
             (ref.at[:, pl.ds(start, n * LANE)], dst.at[slot, :, pl.ds(i * n * LANE, n * LANE)])
             for i, ref in enumerate((g_in, u_in))
@@ -284,12 +286,6 @@
 
     def slot_of(o, zz):
         return zz if o == Q else dev(zz, r)
-
-    started = []
-
-    def launch(cond, make):
-        when(cond, lambda: make().start())
-        started.append((cond, make))
 
     def zsend(o, j):
         return zs.at[o if here[o] is None else chunks + 1 + j]
@@ -344,7 +340,7 @@
 
     def landing(o, j, kind):
         p = psem(o)
-        return pr.at[p, j, 0 if kind == 0 else 1] if kind in (0, 3) else pl_sem.at[p]
+        return pr.at[p, j] if kind in (0, 3) else pl_sem.at[p]
 
     def hop2(o, j, kind):
         owner = (r, r, r, r, rx, ry)[kind]
@@ -352,10 +348,9 @@
         spot = piece(o, j, owner, kind % 2)
         return remote(spot, spot, ps.at[psem(o)], landing(o, j, kind), dev(z, target), t)
 
-    def wait2(o, j, kind):
-        owner = rx if kind == 0 else ry
-        spot = piece(o, j, owner, kind % 2)
-        remote(spot, spot, ps.at[psem(o)], landing(o, j, kind), dev(z, owner), t).wait_recv()
+    def wait2(o, j):
+        spot = store(o).at[dev(behind[j], rx)]
+        remote(spot, spot, ps.at[psem(o)], landing(o, j, 0), dev(z, rx), t).wait_recv()
 
     def spread(o, j):
         if j:
@@ -371,9 +366,8 @@
 
     def relay(o, j):
         def body():
-            wait2(o, j, 0)
+            wait2(o, j)
             hop2(o, j, 4).start()
-            wait2(o, j, 3)
             hop2(o, j, 5).start()
 
         when(here[o], body)
@@ -435,7 +429,7 @@
         return kv_sc[pl.ds(n * R, R), :, first_lane : first_lane + VD].reshape(R * T, VD)
 
     def ho_copy(i):
-        return remote(ho.at[i], heads.at[z], ho_sem.at[0, i], ho_sem.at[1, z], dev(i, r), t)
+        return remote(ho.at[i], heads.at[z], ho_sem.at[Z], ho_sem.at[z], dev(i, r), t)
 
     for i in range(Z):
         ho[i] = attention_block(
@@ -451,7 +445,7 @@
         def _(i=i):
             heads[i] = ho[i]
 
-        launch(z != i, lambda i=i: ho_copy(i))
+        pl.when(z != i)(lambda i=i: ho_copy(i).start())
         if i == 0:
             relay(1, 0)
             spread(0, 1)
@@ -475,7 +469,7 @@
         @pl.when(z != i)
         def _(i=i):
             remote(
-                ho.at[i], heads.at[i], ho_sem.at[0, i], ho_sem.at[1, i], dev(i, r), t
+                ho.at[i], heads.at[i], ho_sem.at[Z], ho_sem.at[i], dev(i, r), t
             ).wait_recv()
 
     first_hop(2, 1)
@@ -528,7 +522,7 @@
     def to_core(down, d, tt):
         rows = rows_of(origin(down, d), tt)
         n = 2 * d + down
-        return remote(rows, rows, core_sem.at[0, n], core_sem.at[1, n], me, 1 - t)
+        return remote(rows, rows, core_sem.at[2 * Z], core_sem.at[n], me, 1 - t)
 
     def ag_start(d):
         for s in range(SUB):
@@ -615,7 +609,7 @@
                 apply(cs, origin(down, d), fresh)
 
     ag_start(1)
-    across = remote(norm_sc, rows_of(z, t), core_sem.at[0, 0], core_sem.at[1, 0], me, 1 - t)
+    across = remote(norm_sc, rows_of(z, t), core_sem.at[2 * Z], core_sem.at[0], me, 1 - t)
     across.start()
     own = pltpu.make_async_copy(norm_sc, rows_of(z, t), local_sem.at[0])
     own.start()
@@ -624,27 +618,30 @@
         first_hop(3, j)
     relay(1, 2)
     spread(2, 1)
-    ag_step(1)
-    own.wait()
-    across.wait_send()
-    remote(
-        norm_sc, rows_of(z, 1 - t), core_sem.at[0, 0], core_sem.at[1, 0], me, 1 - t
-    ).wait_recv()
     spread(2, 2)
     relay(1, 3)
+    settle(0)
+    own.wait()
+    remote(
+        norm_sc, rows_of(z, 1 - t), core_sem.at[2 * Z], core_sem.at[0], me, 1 - t
+    ).wait_recv()
+    apply((0,), z, True)
+    ag_step(1)
     spread(2, 3)
-    for c in early:
-        settle(c)
-    apply(early, z, True)
+    relay(2, 1)
+    ag_done(1)
+    apply_near((0,), 1, True)
+    settle(1)
+    apply((1,), z, False)
     for j in range(1, Z):
         spread(3, j)
-    for j in range(1, Z):
-        relay(2, j)
+    relay(2, 2)
+    relay(2, 3)
+    apply_near((1,), 1, False)
     ag_step(2)
-    ag_done(1)
-    apply_near(early, 1, True)
-    for j in range(1, Z):
-        relay(3, j)
+    relay(3, 1)
+    relay(3, 2)
+    relay(3, 3)
     ag_done(2)
     apply_near(early, 2, True)
     for c in late:
@@ -662,21 +659,21 @@
         seq = [[zd for zd in goal if (zz > zd if down else zz < zd)] for down, goal in enumerate(goals)]
         if zz in (0, Z - 1):
             seq = seq[0] + seq[1]
-            seq = [seq[0]] + seq[2:] + [seq[1]]
+            ranks.append([seq[0]] + seq[2:] + [zz, seq[1]])
         else:
             seq = [zd for k in range(Z - 1) for down in (0, 1) for zd in seq[down][k : k + 1]]
-        ranks.append(seq + [zz])
+            ranks.append(seq + [zz])
 
     def cross_copy(zz):
         return remote(
-            half.at[zz], cross.at[zz], cross_sem.at[0, zz], cross_sem.at[1, zz], me, 1 - t
+            half.at[zz], cross.at[zz], cross_sem.at[Z], cross_sem.at[zz], me, 1 - t
         )
 
     other_rows = pl.ds(pl.multiple_of((1 - t) * H, 16), H)
-    piece = H // SUB
+    small = H // FINE
 
     def rs_copy(down, k, s):
-        rows = pl.ds(s * piece, piece)
+        rows = pl.ds(s * small, small)
         to = z - 1 if down else z + 1
         return remote(
             rs_out.at[down, k, rows],
@@ -688,7 +685,7 @@
         )
 
     def rs_wait(down, k, s):
-        rows = pl.ds(s * piece, piece)
+        rows = pl.ds(s * small, small)
         fro = z + 1 if down else z - 1
         remote(
             rs_out.at[down, k, rows],
@@ -700,18 +697,18 @@
         ).wait_recv()
 
     def mine(zd, s):
-        rows = pl.ds(s * piece, piece)
-        long = pl.ds(pl.multiple_of(t * H + s * piece, 16), piece)
+        rows = pl.ds(s * small, small)
+        long = pl.ds(pl.multiple_of(t * H + s * small, 16), small)
         return acc[zd, long, :] + cross[zd, rows, :].astype(jnp.float32)
 
     def hand_over(zz):
         half[zz] = acc[zz, other_rows, :].astype(jnp.bfloat16)
         cross_copy(zz).start()
 
-    def rs_step(down, k, inner):
+    def rs_step(down, k, inner, subs=range(FINE)):
         zd = goals[down][k]
-        for s in range(SUB):
-            rows = pl.ds(s * piece, piece)
+        for s in subs:
+            rows = pl.ds(s * small, small)
             if s == 0:
                 cross_copy(zd).wait_recv()
             total = mine(zd, s)
@@ -723,13 +720,23 @@
 
     edge = (z == 0) | (z == Z - 1)
 
-    def edge_step(k):
-        pl.when(z == 0)(lambda: rs_step(0, k, False))
-        pl.when(z == Z - 1)(lambda: rs_step(1, k, False))
+    def edge_step(k, low=(0, FINE), high=(0, FINE)):
+        pl.when(z == 0)(lambda: rs_step(0, k, False, range(*low)))
+        pl.when(z == Z - 1)(lambda: rs_step(1, k, False, range(*high)))
+
+    def inner_step(k, subs=range(FINE), lag=0):
+        for half_of, order in ((z < Z // 2, (0, 1)), (z >= Z // 2, (1, 0))):
+            for s in range(subs[0], subs[-1] + 1 + lag):
+                for down, at in zip(order, (s, s - lag)):
+                    if at not in subs:
+                        continue
+                    zd = goals[down][k]
+                    inner = (z > zd) & (z < Z - 1) if down else (z < zd) & (z > 0)
+                    pl.when(half_of & inner)(lambda: rs_step(down, k, True, (at,)))
 
     for n in range(Z):
         zz = pick([ranks[i][n] for i in range(Z)])
-        if n == Z - 2:
+        if n == Z - 1:
             for d in range(3, Z):
                 ag_step(d)
                 ag_done(d)
@@ -740,18 +747,18 @@
         hand_over(zz)
         if n == 1:
             edge_step(0)
+            edge_step(2, (0, 2), (0, 1))
+            inner_step(0, range(FINE // 3))
+        if n == 2:
+            inner_step(0, range(FINE // 3, 2 * FINE // 3))
     edge_step(1)
-    edge_step(2)
-    for half_of, order in ((z < Z // 2, (0, 1)), (z >= Z // 2, (1, 0))):
-        for k in range(Z - 1):
-            for down in order:
-                zd = goals[down][k]
-                inner = (z > zd) & (z < Z - 1) if down else (z < zd) & (z > 0)
-                pl.when(half_of & inner)(lambda: rs_step(down, k, True))
+    edge_step(2, (2, FINE), (1, FINE))
+    inner_step(0, range(2 * FINE // 3, FINE))
+    for k in range(1, Z - 1):
+        inner_step(k, range(FINE), 2)
     cross_copy(z).wait_recv()
-    ends = []
-    for s in range(SUB):
-        rows = pl.ds(s * piece, piece)
+    for s in range(FINE):
+        rows = pl.ds(s * small, small)
         first[rows, :] = first[rows, :] + 0.5 * mine(z, s)
         for down in (0, 1):
 
@@ -762,23 +769,16 @@
                 first[rows, :] = first[rows, :] + 0.5 * rs_in[down, k, rows, :].astype(jnp.float32)
 
         res[rows, :] = first[rows, :].astype(jnp.bfloat16)
-        place = out.at[pl.ds(pl.multiple_of(t * H + s * piece, 16), piece), :]
-        c = remote(res.at[rows], place, out_sem.at[0, s], out_sem.at[1, s], me, 1 - t)
-        c.start()
-        ends.append(c)
-        c = pltpu.make_async_copy(res.at[rows], place, local_sem.at[1 + s])
-        c.start()
-        ends.append(c)
-    for c in ends:
-        c.wait()
-    for zz in range(Z):
-        cross_copy(zz).wait_send()
+        place = out.at[pl.ds(pl.multiple_of(t * H + s * small, 16), small), :]
+        remote(res.at[rows], place, out_sem.at[0], out_sem.at[1], me, 1 - t).start()
+        pltpu.make_async_copy(res.at[rows], place, local_sem.at[1]).start()
+    theirs = out.at[pl.ds(pl.multiple_of((1 - t) * H, 16), H), :]
+    remote(res, theirs, out_sem.at[0], out_sem.at[1], me, 1 - t).wait()
+    pltpu.make_async_copy(res, out.at[own_rows, :], local_sem.at[1]).wait()
+    remote(half, cross, cross_sem.at[Z], cross_sem.at[0], me, 1 - t).wait_send()
+    remote(half, cross, core_sem.at[2 * Z], core_sem.at[0], me, 1 - t).wait_send()
     for d in range(1, Z):
         for down in (0, 1):
-
-            @pl.when(gets(down, d))
-            def _(down=down, d=d):
-                to_core(down, d, t).wait_send()
 
             @pl.when(sends(down, d))
             def _(down=down, d=d):
@@ -797,8 +797,8 @@
         first_hops_sent(o)
     for o in (KV, *range(chunks)):
         spread_sent(o)
-    for cond, make in started:
-        when(cond, lambda make=make: make().wait_send())
+    sent = ho.at[pl.ds(0, Z - 1)]
+    remote(sent, sent, ho_sem.at[Z], ho_sem.at[0], me, 1 - t).wait_send()
 
 
 def columns_form(
@@ -835,7 +835,7 @@
 
     return pl.pallas_call(
         kernel,
-        out_shape=jax.ShapeDtypeStruct((T, D), bf),
+        out_shape=pltpu.VMEM((T, D), bf),
         in_specs=[hbm] * 8 + [pl.BlockSpec(memory_space=pltpu.SMEM), vm, vm],
         out_specs=vm,
         scratch_shapes=[
@@ -862,18 +862,18 @@
             dma((chunks + 1 + Z,)),
             dma((chunks + 2, Z - 1)),
             dma((chunks + 1,)),
-            dma((chunks + 1, Z, 2)),
+            dma((chunks + 1, Z)),
             dma((chunks + 1,)),
             dma((chunks + 4,)),
-            dma((2, Z)),
+            dma((Z + 1,)),
             dma((2,)),
             dma((2, Z)),
             dma((2, Z, SUB)),
-            dma((2, 2 * Z)),
-            dma((2, Z)),
+            dma((2 * Z + 1,)),
+            dma((Z + 1,)),
             dma((2, Z - 1)),
-            dma((2, Z - 1, SUB)),
-            dma((2, SUB)),
+            dma((2, Z - 1, FINE)),
+            dma((2,)),
         ],
         compiler_params=pltpu.CompilerParams(
             collective_id=0, has_side_effects=True, vmem_limit_bytes=VMEM_LIMIT
@@ -908,7 +908,8 @@
             and args[8].shape[1] % LANE == 0
             and args[8].shape[1] // LANE // heads == 5
             and args[8].shape[1] // LANE % heads != 0
-            and tok_rows % (32 * SUB) == 0
+            and tok_rows % (32 * FINE) == 0
+            and FINE % SUB == 0
         )
         return (columns_form if columns else generic)(*args)
 

time: 134 us -> 129 us (0.963)
  Pallas kernels: 132 us -> 128 us
    pallas_call x1, Pallas kernels: 132 us -> 128 us  [columns_form(): pl.pallas_call(kernel, out_shape=pltpu.VMEM((T, D), bf), in_specs=[hbm] *...]
where the time goes in v3:
time: 129 us
  Pallas kernels  128 us (99%)
    pallas_call x1, Pallas kernels, columns_form(): pl.pallas_call(kernel, out_shape=pltpu.VMEM((T, D), bf), in_specs=[hbm] *...  128 us

profile of v3, /device:TPU:0, one launch (start us, length us, event | category | flops | bytes accessed | tf_op | source)
XLA Modules:
  0.0 129.1 jit_solution(10535462208886404578)
XLA Ops:
  0.0 128.2 %shard_map.109 = bf16[192,2048]{1,0:T(8,128)(2,1)S(1)} custom-call(bf16[192,512]{1,0:T(8,128)(2,1)} %refs_0_.1, bf16[192,512]{1,0:T(8,128)(2,1)} %refs_1_.1, bf16[192,512]{1,0:T(8,128)(2,1)} %refs_2_.1, bf16[128,2816]{1,0:T(8,128)(2,1)} %refs_3_.1, bf16[128,2816]{1,0:T(8,128)(2,1)} %refs_4_.1, bf16[2816,128]{1,0:T(8,128)(2,1)} %refs_5_.1, ...), custom_call_target="tpu_custom_call" | custom-call | tf_op jit(solution)/shard_map/pallas_call | solution.py:836
  128.2 0.9 copy.13

commit v4 on v3

--- a/solution.py
+++ b/solution.py
@@ -401,7 +401,7 @@
         [(dev(ahead[j], r), t) for j in range(1, Z)]
         + [(dev(z, rx), t), (dev(z, ry), t), (me, 1 - t)]
     )
-    for o in (KV, Q, 0, 1):
+    for o in (KV, 0, Q, 1):
         for j in range(1, Z):
             first_hop(o, j)
         if o == KV:
@@ -419,6 +419,12 @@
     for c in range(2, chunks):
         spread(c, 0)
     settle(KV)
+    relay(1, 0)
+    spread(0, 1)
+    relay(2, 0)
+    relay(3, 0)
+    spread(0, 2)
+    relay(0, 1)
     kept(Q)
     for j in range(1, Z):
         arrived(Q, j)
@@ -446,17 +452,10 @@
             heads[i] = ho[i]
 
         pl.when(z != i)(lambda i=i: ho_copy(i).start())
-        if i == 0:
-            relay(1, 0)
-            spread(0, 1)
         if i == 1:
-            relay(2, 0)
-            relay(3, 0)
+            spread(0, 3)
         if i == 2:
-            spread(0, 2)
-            relay(0, 1)
-    spread(0, 3)
-    relay(0, 2)
+            relay(0, 2)
     spread(1, 1)
     spread(1, 2)
     relay(0, 3)
@@ -474,6 +473,7 @@
 
     first_hop(2, 1)
     first_hop(2, 2)
+    pl.when(z == 0)(lambda: first_hop(2, 3))
     NT = 512 if D % 512 == 0 else D
     for h in range(2):
         hh = (1 - t) if h == 0 else t
@@ -592,15 +592,6 @@
     early = tuple(range(pairs))
     late = tuple(range(pairs, chunks))
 
-    def apply_last(cs, zz, fresh):
-        cond = here[chunks - 1]
-        if cond is None:
-            apply(cs, zz, fresh)
-            return
-        pl.when(cond)(lambda: apply(cs, zz, fresh))
-        if cs[:-1]:
-            pl.when(jnp.logical_not(cond))(lambda: apply(cs[:-1], zz, fresh))
-
     def apply_near(cs, d, fresh):
         for down in (0, 1):
 
@@ -613,7 +604,7 @@
     across.start()
     own = pltpu.make_async_copy(norm_sc, rows_of(z, t), local_sem.at[0])
     own.start()
-    first_hop(2, 3)
+    pl.when(z > 0)(lambda: first_hop(2, 3))
     for j in range(1, Z):
         first_hop(3, j)
     relay(1, 2)
@@ -631,38 +622,28 @@
     relay(2, 1)
     ag_done(1)
     apply_near((0,), 1, True)
+    spread(3, 1)
+    spread(3, 2)
+    relay(2, 2)
+    spread(3, 3)
+    relay(2, 3)
     settle(1)
     apply((1,), z, False)
-    for j in range(1, Z):
-        spread(3, j)
-    relay(2, 2)
-    relay(2, 3)
     apply_near((1,), 1, False)
     ag_step(2)
     relay(3, 1)
     relay(3, 2)
     relay(3, 3)
-    ag_done(2)
-    apply_near(early, 2, True)
-    for c in late:
-        settle(c)
-
     def pick(table):
         spot = jnp.int32(0)
         for zz in range(Z):
             spot = jnp.where(z == zz, table[zz], spot)
         return spot
 
-    goals = [[Z - 2, Z - 1] + list(range(Z - 3, 0, -1)), [1, 0] + list(range(2, Z - 1))]
-    ranks = []
-    for zz in range(Z):
-        seq = [[zd for zd in goal if (zz > zd if down else zz < zd)] for down, goal in enumerate(goals)]
-        if zz in (0, Z - 1):
-            seq = seq[0] + seq[1]
-            ranks.append([seq[0]] + seq[2:] + [zz, seq[1]])
-        else:
-            seq = [zd for k in range(Z - 1) for down in (0, 1) for zd in seq[down][k : k + 1]]
-            ranks.append(seq + [zz])
+    goals = [[1, Z - 1, *range(2, Z - 1)], [Z - 2, 0, *range(Z - 3, 0, -1)]]
+    ranks = [[2, 3, 0, 1], [1, 0, 3, 2]]
+    edge = (z == 0) | (z == Z - 1)
+    fill = (3, 1)
 
     def cross_copy(zz):
         return remote(
@@ -718,44 +699,61 @@
             rs_out[down, k, rows, :] = total.astype(jnp.bfloat16)
             rs_copy(down, k, s).start()
 
-    edge = (z == 0) | (z == Z - 1)
-
     def edge_step(k, low=(0, FINE), high=(0, FINE)):
         pl.when(z == 0)(lambda: rs_step(0, k, False, range(*low)))
         pl.when(z == Z - 1)(lambda: rs_step(1, k, False, range(*high)))
 
-    def inner_step(k, subs=range(FINE), lag=0):
-        for half_of, order in ((z < Z // 2, (0, 1)), (z >= Z // 2, (1, 0))):
-            for s in range(subs[0], subs[-1] + 1 + lag):
-                for down, at in zip(order, (s, s - lag)):
-                    if at not in subs:
-                        continue
-                    zd = goals[down][k]
-                    inner = (z > zd) & (z < Z - 1) if down else (z < zd) & (z > 0)
-                    pl.when(half_of & inner)(lambda: rs_step(down, k, True, (at,)))
-
-    for n in range(Z):
-        zz = pick([ranks[i][n] for i in range(Z)])
-        if n == Z - 1:
-            for d in range(3, Z):
-                ag_step(d)
-                ag_done(d)
-            pl.when(edge)(lambda: apply_last(early + late, zz, True))
-            pl.when(jnp.logical_not(edge))(lambda: apply_last(late, zz, False))
-        else:
-            apply_last(late, zz, False)
-        hand_over(zz)
-        if n == 1:
-            edge_step(0)
-            edge_step(2, (0, 2), (0, 1))
-            inner_step(0, range(FINE // 3))
-        if n == 2:
-            inner_step(0, range(FINE // 3, 2 * FINE // 3))
-    edge_step(1)
-    edge_step(2, (2, FINE), (1, FINE))
-    inner_step(0, range(2 * FINE // 3, FINE))
-    for k in range(1, Z - 1):
-        inner_step(k, range(FINE), 2)
+    @pl.when(edge)
+    def _():
+        settle(2)
+        near = jnp.where(z == 0, 1, Z - 2)
+        apply((2,), near, False)
+        hand_over(near)
+
+    ag_done(2)
+    apply_near(early, 2, True)
+
+    @pl.when(edge)
+    def _():
+        edge_step(0)
+        mid = jnp.where(z == 0, 2, Z - 3)
+        apply((2,), mid, False)
+        hand_over(mid)
+        apply((2,), z, False)
+        hand_over(z)
+        edge_step(2, (0, fill[0]), (0, fill[1]))
+        for d in range(3, Z):
+            ag_step(d)
+            ag_done(d)
+        far = jnp.where(z == 0, Z - 1, 0)
+        apply(early + (2,), far, True)
+        hand_over(far)
+        edge_step(1)
+        edge_step(2, (fill[0], FINE), (fill[1], FINE))
+
+    @pl.when(jnp.logical_not(edge))
+    def _():
+        for c in late:
+            settle(c)
+        for n in range(Z):
+            zz = jnp.where(z == 1, ranks[0][n], ranks[1][n])
+            apply(late, zz, False)
+            hand_over(zz)
+        for low in (True, False):
+
+            @pl.when(z == 1 if low else z == 2)
+            def _(low=low):
+                count = fill[0] if low else fill[1]
+                first_way, second_way = (0, 1) if low else (1, 0)
+                rs_step(first_way, 2, True, range(count))
+                for s in range(FINE + 2):
+                    if s < FINE:
+                        rs_step(first_way, 1, True, (s,))
+                    if s >= 2:
+                        rs_step(second_way, 1, True, (s - 2,))
+                rs_step(first_way, 2, True, range(count, FINE))
+
+
     cross_copy(z).wait_recv()
     for s in range(FINE):
         rows = pl.ds(s * small, small)
@@ -907,7 +905,7 @@
             and args[8].shape[0] == LANE
             and args[8].shape[1] % LANE == 0
             and args[8].shape[1] // LANE // heads == 5
-            and args[8].shape[1] // LANE % heads != 0
+            and args[8].shape[1] // LANE % heads == 2
             and tok_rows % (32 * FINE) == 0
             and FINE % SUB == 0
         )

time: 129 us -> 128 us (level)
  the two profiles are of different devices: /device:TPU:0 before, /device:TPU:9 now
where the time goes in v4:
time: 128 us
  Pallas kernels  127 us (99%)
    pallas_call x1, Pallas kernels, columns_form(): pl.pallas_call(kernel, out_shape=pltpu.VMEM((T, D), bf), in_specs=[hbm] *...  127 us

profile of v4, /device:TPU:9, one launch (start us, length us, event | category | flops | bytes accessed | tf_op | source)
XLA Modules:
  0.0 128.3 jit_solution(2961582959726268777)
XLA Ops:
  0.0 127.4 %shard_map.109 = bf16[192,2048]{1,0:T(8,128)(2,1)S(1)} custom-call(bf16[192,512]{1,0:T(8,128)(2,1)} %refs_0_.1, bf16[192,512]{1,0:T(8,128)(2,1)} %refs_1_.1, bf16[192,512]{1,0:T(8,128)(2,1)} %refs_2_.1, bf16[128,2816]{1,0:T(8,128)(2,1)} %refs_3_.1, bf16[128,2816]{1,0:T(8,128)(2,1)} %refs_4_.1, bf16[2816,128]{1,0:T(8,128)(2,1)} %refs_5_.1, ...), custom_call_target="tpu_custom_call" | custom-call | tf_op jit(solution)/shard_map/pallas_call | solution.py:834
  127.4 0.9 copy.13

commit v5 on v4

--- a/solution.py
+++ b/solution.py
@@ -456,11 +456,11 @@
             spread(0, 3)
         if i == 2:
             relay(0, 2)
+    first_hop(2, 1)
+    first_hop(2, 2)
     spread(1, 1)
     spread(1, 2)
     relay(0, 3)
-    spread(1, 3)
-    relay(1, 1)
     resid_copy.wait()
     w_copy.wait()
     for i in range(Z):
@@ -471,8 +471,6 @@
                 ho.at[i], heads.at[i], ho_sem.at[Z], ho_sem.at[i], dev(i, r), t
             ).wait_recv()
 
-    first_hop(2, 1)
-    first_hop(2, 2)
     pl.when(z == 0)(lambda: first_hop(2, 3))
     NT = 512 if D % 512 == 0 else D
     for h in range(2):
@@ -607,6 +605,8 @@
     pl.when(z > 0)(lambda: first_hop(2, 3))
     for j in range(1, Z):
         first_hop(3, j)
+    spread(1, 3)
+    relay(1, 1)
     relay(1, 2)
     spread(2, 1)
     spread(2, 2)
@@ -643,7 +643,7 @@
     goals = [[1, Z - 1, *range(2, Z - 1)], [Z - 2, 0, *range(Z - 3, 0, -1)]]
     ranks = [[2, 3, 0, 1], [1, 0, 3, 2]]
     edge = (z == 0) | (z == Z - 1)
-    fill = (3, 1)
+    fill = (3, 2)
 
     def cross_copy(zz):
         return remote(

time: 128 us -> 127 us (level)
  the two profiles are of different devices: /device:TPU:9 before, /device:TPU:0 now
where the time goes in v5:
time: 127 us; the launch traced here: 125 us
  Pallas kernels  124 us (98%)
    pallas_call x1, Pallas kernels, columns_form(): pl.pallas_call(kernel, out_shape=pltpu.VMEM((T, D), bf), in_specs=[hbm] *...  124 us

profile of v5, /device:TPU:0, one launch (start us, length us, event | category | flops | bytes accessed | tf_op | source)
XLA Modules:
  0.0 125.0 jit_solution(15531139087417545322)
XLA Ops:
  0.0 124.1 %shard_map.109 = bf16[192,2048]{1,0:T(8,128)(2,1)S(1)} custom-call(bf16[192,512]{1,0:T(8,128)(2,1)} %refs_0_.1, bf16[192,512]{1,0:T(8,128)(2,1)} %refs_1_.1, bf16[192,512]{1,0:T(8,128)(2,1)} %refs_2_.1, bf16[128,2816]{1,0:T(8,128)(2,1)} %refs_3_.1, bf16[128,2816]{1,0:T(8,128)(2,1)} %refs_4_.1, bf16[2816,128]{1,0:T(8,128)(2,1)} %refs_5_.1, ...), custom_call_target="tpu_custom_call" | custom-call | tf_op jit(solution)/shard_map/pallas_call | solution.py:834
  124.1 0.9 copy.13
